TPU v7x, 32 devices: a whole 2x2x4 slice. The times are simulated.
32 devices in a mesh: sp: 8 (over z, y), tp: 4 (over x, core).
Axes of the slice: x: 2, y: 2, z: 4, core: 2. Of those that a mesh axis runs over, the one named last changes fastest.
Arguments:
- target: bfloat16 [2048, 2048], P(('sp', 'tp')), may hold values from -6 to 6
- source: bfloat16 [4096, 2048], P(('sp', 'tp')), may hold values from -6 to 6
- target_gain: bfloat16 [2, 2048], replicated, may hold values from 0.099609375 to 1.8984375
- source_gain: bfloat16 [2, 2048], replicated, may hold values from 0.099609375 to 1.8984375
- query_w: bfloat16 [2, 2048, 8192], P(None, None, 'tp'), may hold values from -0.125 to 0.125
- key_w: bfloat16 [2, 2048, 4096], P(None, None, 'tp'), may hold values from -0.125 to 0.125
- value_w: bfloat16 [2, 2048, 4096], P(None, None, 'tp'), may hold values from -0.125 to 0.125
- out_w: bfloat16 [2, 8192, 2048], P(None, 'tp'), may hold values from -0.1875 to 0.1875
- head_temp: float32 [2, 16], P(None, 'tp'), may hold values from 1.5 to 8, as said below
- final_gain: bfloat16 [2048], replicated, may hold values from 0.099609375 to 1.8984375
Outputs:
- result: float32 [2048, 2048], P(('sp', 'tp'))
Inputs may be any that keep to these rules, and one draw needn't show every extreme that they name: `head_temp`: a positive scale for each head's scores.
All inputs are finite; a program needn't handle non-finite values.
Results may differ from a plain program's by a relative error of at most 0.04.
Values may be sent and summed in bfloat16 or wider, within the bound.
A program may use at most 192 MiB of HBM per device.

v0:
```python
import functools
import math

import jax
import jax.numpy as jnp
from jax import lax
from jax.experimental import pallas as pl
from jax.experimental.pallas import tpu as pltpu
from jax.sharding import PartitionSpec as P

HEAD_DIM = 512
EPS = 1e-06
FLOOR = -1e30
CHUNK = 512
ROWS = 512
LOG2E = math.log2(math.e)


def unit_rows(matrix):
    values = matrix.astype(jnp.float32)
    return values * lax.rsqrt(jnp.mean(values * values, axis=-1, keepdims=True) + EPS)


def shifted(block, shift):
    size = lax.axis_size("tp")
    return lax.ppermute(block, "tp", [(i, (i + shift) % size) for i in range(size)])


def gather_rows(block):
    size = lax.axis_size("tp")
    return jnp.concatenate([block] + [shifted(block, k) for k in range(1, size)], axis=0)


def return_rows(blocks):
    size = lax.axis_size("tp")
    count = blocks.shape[0] // size
    mixed = blocks[:count].astype(jnp.float32)
    for k in range(1, size):
        mixed += shifted(blocks[k * count : (k + 1) * count], -k).astype(jnp.float32)
    return mixed


def attend_kernel(rows, query_ref, source_ref, mix_ref, total_ref, top_ref, sum_ref):
    step = pl.program_id(0)
    count = query_ref.shape[0]

    @pl.when(step == 0)
    def _():
        total_ref[...] = jnp.zeros_like(total_ref)
        sum_ref[...] = jnp.zeros_like(sum_ref)
        top_ref[...] = jnp.full_like(top_ref, FLOOR)

    for start in range(0, count, rows):
        block = pl.ds(start, rows)
        scores = lax.dot_general(
            query_ref[block, :],
            source_ref[...],
            (((1,), (1,)), ((), ())),
            preferred_element_type=jnp.float32,
        )
        old_top = top_ref[block, :1]
        new_top = jnp.maximum(old_top, jnp.max(scores, axis=-1, keepdims=True))
        shrink = jnp.exp2(old_top - new_top)
        expo = jnp.exp2(scores - new_top)
        top_ref[block, :] = jnp.broadcast_to(new_top, (rows, top_ref.shape[1]))
        new_sum = sum_ref[block, :1] * shrink + jnp.sum(expo, axis=-1, keepdims=True)
        sum_ref[block, :] = jnp.broadcast_to(new_sum, (rows, sum_ref.shape[1]))
        total_ref[block, :] = total_ref[block, :] * shrink + jnp.dot(
            expo.astype(jnp.bfloat16), source_ref[...], preferred_element_type=jnp.float32
        )

    @pl.when(step == pl.num_programs(0) - 1)
    def _():
        for start in range(0, count, rows):
            block = pl.ds(start, rows)
            mix_ref[block, :] = (total_ref[block, :] / sum_ref[block, :1]).astype(mix_ref.dtype)


def attend(query, source, chunk=CHUNK, rows=ROWS):
    count, width = query.shape
    positions = source.shape[0]
    chunk = math.gcd(chunk, positions)
    rows = math.gcd(rows, count)
    return pl.pallas_call(
        functools.partial(attend_kernel, rows),
        grid=(positions // chunk,),
        out_shape=jax.ShapeDtypeStruct((count, width), jnp.bfloat16),
        in_specs=[
            pl.BlockSpec((count, width), lambda j: (0, 0), pipeline_mode=pl.Buffered(1)),
            pl.BlockSpec((chunk, width), lambda j: (j, 0)),
        ],
        out_specs=pl.BlockSpec((count, width), lambda j: (0, 0), pipeline_mode=pl.Buffered(1)),
        scratch_shapes=[
            pltpu.VMEM((count, width), jnp.float32),
            pltpu.VMEM((count, 128), jnp.float32),
            pltpu.VMEM((count, 128), jnp.float32),
        ],
        compiler_params=pltpu.CompilerParams(
            dimension_semantics=("arbitrary",), vmem_limit_bytes=56 * 1024 * 1024
        ),
        cost_estimate=pl.CostEstimate(
            flops=4 * count * positions * width,
            bytes_accessed=2 * positions * width,
            transcendentals=count * positions,
        ),
    )(query, source)


def per_device(
    target, source, target_gain, source_gain, query_w, key_w, value_w, out_w, head_temp, final_gain
):
    width = target.shape[1]
    heads = query_w.shape[2] // HEAD_DIM
    shared = key_w.shape[2] // HEAD_DIM
    group = heads // shared
    positions = lax.all_gather(
        unit_rows(source).astype(jnp.bfloat16), ("sp", "tp"), axis=0, tiled=True
    )
    hidden_state = target.astype(jnp.float32)
    for layer in range(2):
        gain = source_gain[layer].astype(jnp.float32)
        normed = (unit_rows(hidden_state) * target_gain[layer].astype(jnp.float32)).astype(
            jnp.bfloat16
        )
        queries = jnp.dot(
            gather_rows(normed),
            query_w[layer],
            preferred_element_type=jnp.float32,
        ).astype(jnp.bfloat16)
        count = queries.shape[0]
        scales = head_temp[layer] * (HEAD_DIM ** (-0.5) * LOG2E)
        lifted = []
        for head in range(heads):
            columns = slice((head // group) * HEAD_DIM, (head // group + 1) * HEAD_DIM)
            lifted.append(
                (
                    lax.dot_general(
                        queries[:, head * HEAD_DIM : (head + 1) * HEAD_DIM],
                        key_w[layer][:, columns],
                        (((1,), (1,)), ((), ())),
                        preferred_element_type=jnp.float32,
                    )
                    * (gain * scales[head])
                ).astype(jnp.bfloat16)
            )
        mix = attend(jnp.concatenate(lifted, axis=0), positions)
        attended = []
        for head in range(heads):
            columns = slice((head // group) * HEAD_DIM, (head // group + 1) * HEAD_DIM)
            own = (mix[head * count : (head + 1) * count].astype(jnp.float32) * gain).astype(
                jnp.bfloat16
            )
            attended.append(
                jnp.dot(
                    own, value_w[layer][:, columns], preferred_element_type=jnp.float32
                ).astype(jnp.bfloat16)
            )
        mixed = return_rows(
            jnp.dot(
                jnp.concatenate(attended, axis=1),
                out_w[layer],
                preferred_element_type=jnp.float32,
            ).astype(jnp.bfloat16)
        )
        hidden_state = hidden_state + mixed
    return unit_rows(hidden_state) * final_gain.astype(jnp.float32)


def solution(mesh):
    in_specs = (
        P(("sp", "tp"), None),
        P(("sp", "tp"), None),
        P(),
        P(),
        P(None, None, "tp"),
        P(None, None, "tp"),
        P(None, None, "tp"),
        P(None, "tp", None),
        P(None, "tp"),
        P(),
    )
    out_specs = P(("sp", "tp"), None)
    return jax.shard_map(
        per_device, mesh=mesh, in_specs=in_specs, out_specs=out_specs, check_vma=False
    )
```

profile of v0, /device:TPU:0, one launch (start us, length us, event | category | flops | bytes accessed | tf_op | source)
XLA Modules:
  0.0 322.0 jit_solution(13396255774953966462)
XLA Ops:
  6.6 1.3 fusion.80
  7.9 2.0 fusion.81
  10.8 2.6 collective-permute-start.1
  13.3 1.4 collective-permute-start.2
  15.4 4.9 %broadcast_multiply_fusion.3 = (f32[1,2048]{1,0:T(1,128)S(1)}, f32[1,2048]{1,0:T(1,128)S(1)}, f32[1,2048]{1,0:T(1,128)S(1)}, f32[1,2048]{1,0:T(1,128)S(1)}, f32[...) fusion(f32[]{:T(128)} %bitcast.17, ...), kind=kLoop, calls=%fused_computation.152 | loop fusion | flops 20480 | bytes 73760 | tf_op jit(solution)/shard_map/mul | solution.py:143
  20.3 5.9 %slice_bitcast_fusion.1 = (bf16[2048,1024]{1,0:T(8,128)(2,1)}, bf16[2048,1024]{1,0:T(8,128)(2,1)S(1)}) fusion(bf16[2,2048,1024]{2,1,0:T(8,128)(2,1)} %param.15), kind=kLoop, calls=%fused_computation.15 | loop fusion | bytes 16777216 | tf_op jit(solution)/shard_map/squeeze | solution.py:139
  26.9 4.6 %slice_bitcast_fusion = (bf16[2048,1024]{1,0:T(8,128)(2,1)}, bf16[2048,1024]{1,0:T(8,128)(2,1)}) fusion(bf16[2,2048,1024]{2,1,0:T(8,128)(2,1)S(1)} %bitcast.49), kind=kLoop, calls=%fused_computation.14 | loop fusion | bytes 16777216 | tf_op jit(solution)/shard_map/squeeze | solution.py:155
  31.5 4.1 %copy-done.8 = bf16[2,2048,2048]{2,1,0:T(8,128)(2,1)S(1)} copy-done((bf16[2,2048,2048]{2,1,0:T(8,128)(2,1)S(1)}, bf16[2,2048,2048]{2,1,0:T(8,128)(2,1)}, u32[]{:S(2)}) %copy-start.8) | copy-done | bytes 16777240
  35.6 2.4 fusion.20
  41.0 2.3 pad_maximum_fusion.query_ref
  43.4 85.9 %all-gather.2.cloned.1.call-done.source_ref = bf16[4096,2048]{1,0:T(8,128)(2,1)} async-done(((bf16[128,2048]{1,0:T(8,128)(2,1)}), bf16[4096,2048]{1,0:T(8,128)(2,1)}) %all-gather.2.cloned.1.call-update) | async-done | bytes 16777232 | tf_op jit(solution)/shard_map/all_gather | solution.py:116
  129.2 56.0 %shard_map.100 = bf16[1024,2048]{1,0:T(8,128)(2,1)} custom-call(bf16[1024,2048]{1,0:T(8,128)(2,1)} %pad_maximum_fusion.query_ref, bf16[4096,2048]{1,0:T(8,128)(2,1)} %all-gather.2.cloned.1.call-done.source_ref), custom_call_target="tpu_custom_call" | custom-call | flops 34359738368 | bytes 16777216 | tf_op jit(solution)/shard_map/pallas_call | solution.py:84
  185.2 2.1 fusion.56
  190.0 6.4 %fusion.23 = bf16[256,2048]{1,0:T(8,128)(2,1)S(1)} fusion(bf16[2,2048,2048]{2,1,0:T(8,128)(2,1)} %param.17, bf16[256,512]{1,0:T(8,128)(2,1)S(1)} %fusion.65, bf16[256,512]{1,0:T(8,128)(2,1)S(1)} %fusion.62, bf16[256,512]{1,0:T(8,128)(2,1)S(1)} %fusion.59, bf16[256,512]{1,0:T(8,128)(2,1)S(1)} %fusion.56), kind=kOutput, calls=%fused_computation.35 | convolution fusion | flops 2152202240 | bytes 10485760 | tf_op jit(solution)/shard_map/dot_general | solution.py:159
  196.5 1.2 collective-permute-start.3
  198.4 5.9 %collective-permute-done.3 = bf16[64,2048]{1,0:T(8,128)(2,1)S(1)} collective-permute-done((bf16[64,2048]{1,0:T(8,128)(2,1)S(1)}, bf16[64,2048]{1,0:T(8,128)(2,1)S(1)}, u32[]{:S(2)}, u32[]{:S(2)}) %collective-permute-start.3) | collective-permute-done | bytes 262176 | tf_op jit(solution)/shard_map/ppermute | solution.py:26
  204.4 6.5 %collective-permute-done.4 = bf16[64,2048]{1,0:T(8,128)(2,1)S(1)} collective-permute-done((bf16[64,2048]{1,0:T(8,128)(2,1)S(1)}, bf16[64,2048]{1,0:T(8,128)(2,1)S(1)}, u32[]{:S(2)}, u32[]{:S(2)}) %collective-permute-start.4) | collective-permute-done | bytes 262176 | tf_op jit(solution)/shard_map/ppermute | solution.py:26
  211.4 1.3 collective-permute-start.7
  212.7 1.4 collective-permute-start.8
  214.1 5.2 %collective-permute-done.6 = bf16[64,2048]{1,0:T(8,128)(2,1)S(1)} collective-permute-done((bf16[64,2048]{1,0:T(8,128)(2,1)S(1)}, bf16[64,2048]{1,0:T(8,128)(2,1)S(1)}, u32[]{:S(2)}, u32[]{:S(2)}) %collective-permute-start.6) | collective-permute-done | bytes 262176 | tf_op jit(solution)/shard_map/ppermute | solution.py:26
  219.3 1.3 collective-permute-done.7
  220.7 3.7 %collective-permute-done.8 = bf16[64,2048]{1,0:T(8,128)(2,1)S(1)} collective-permute-done((bf16[64,2048]{1,0:T(8,128)(2,1)S(1)}, bf16[64,2048]{1,0:T(8,128)(2,1)S(1)}, u32[]{:S(2)}, u32[]{:S(2)}) %collective-permute-start.8) | collective-permute-done | bytes 262176 | tf_op jit(solution)/shard_map/ppermute | solution.py:26
  224.4 2.4 fusion.26
  229.9 2.5 pad_maximum_fusion.1.query_ref
  232.4 56.0 %shard_map.101 = bf16[1024,2048]{1,0:T(8,128)(2,1)} custom-call(bf16[1024,2048]{1,0:T(8,128)(2,1)} %pad_maximum_fusion.1.query_ref, bf16[4096,2048]{1,0:T(8,128)(2,1)} %all-gather.2.cloned.1.call-done.source_ref), custom_call_target="tpu_custom_call" | custom-call | flops 34359738368 | bytes 16777216 | tf_op jit(solution)/shard_map/pallas_call | solution.py:84
  288.4 2.1 fusion.68
  293.2 5.7 %fusion.29 = bf16[256,2048]{1,0:T(8,128)(2,1)S(1)} fusion(bf16[2,2048,2048]{2,1,0:T(8,128)(2,1)} %param.17, bf16[256,512]{1,0:T(8,128)(2,1)S(1)} %fusion.77, bf16[256,512]{1,0:T(8,128)(2,1)S(1)} %fusion.74, bf16[256,512]{1,0:T(8,128)(2,1)S(1)} %fusion.71, bf16[256,512]{1,0:T(8,128)(2,1)S(1)} %fusion.68), kind=kOutput, calls=%fused_computation.37 | convolution fusion | flops 2152202240 | bytes 10485760 | tf_op jit(solution)/shard_map/dot_general | solution.py:159
  299.0 0.8 collective-permute-start.10
  299.8 1.3 collective-permute-start.11
  301.6 6.6 %collective-permute-done.10 = bf16[64,2048]{1,0:T(8,128)(2,1)S(1)} collective-permute-done((bf16[64,2048]{1,0:T(8,128)(2,1)S(1)}, bf16[64,2048]{1,0:T(8,128)(2,1)S(1)}, u32[]{:S(2)}, u32[]{:S(2)}) %collective-permute-start.10) | collective-permute-done | bytes 262176 | tf_op jit(solution)/shard_map/ppermute | solution.py:26
  308.1 5.7 %collective-permute-done.11 = bf16[64,2048]{1,0:T(8,128)(2,1)S(1)} collective-permute-done((bf16[64,2048]{1,0:T(8,128)(2,1)S(1)}, bf16[64,2048]{1,0:T(8,128)(2,1)S(1)}, u32[]{:S(2)}, u32[]{:S(2)}) %collective-permute-start.11) | collective-permute-done | bytes 262176 | tf_op jit(solution)/shard_map/ppermute | solution.py:26
  314.1 1.0 multiply_multiply_fusion
  (77 shorter events, 15.8 us)
Async XLA Ops:
  6.5 3.3 %copy-start.3 = (bf16[64,2048]{1,0:T(8,128)(2,1)S(1)}, bf16[64,2048]{1,0:T(8,128)(2,1)}, u32[]{:S(2)}) copy-start(bf16[64,2048]{1,0:T(8,128)(2,1)} %param.10) | copy-start | bytes 786436
  6.5 3.5 %copy-start.5 = (bf16[2,2048]{1,0:T(2,128)(2,1)S(1)}, bf16[2,2048]{1,0:T(2,128)(2,1)}, u32[]{:S(2)}) copy-start(bf16[2,2048]{1,0:T(2,128)(2,1)} %param.12) | copy-start | bytes 24580
  6.5 8.2 %copy-start.7 = (f32[2,4]{1,0:T(2,128)S(1)}, f32[2,4]{1,0:T(2,128)}, u32[]{:S(2)}) copy-start(f32[2,4]{1,0:T(2,128)} %param.18) | copy-start | bytes 100
  6.5 8.9 %copy-start.4 = (bf16[2,2048]{1,0:T(2,128)(2,1)S(1)}, bf16[2,2048]{1,0:T(2,128)(2,1)}, u32[]{:S(2)}) copy-start(bf16[2,2048]{1,0:T(2,128)(2,1)} %param.13) | copy-start | bytes 24580
  6.5 122.7 %all-gather.2.cloned.1.call-start = ((), (), s32[]{:S(2)}) async-start(), calls=%async_computation | async-start | bytes 17301504 | tf_op jit(solution)/shard_map/all_gather | solution.py:116
  10.1 16.1 %slice-start = ((s8[8388608]{0:T(1024)(128)(4,1)}), s8[4194304]{0:T(1024)(128)(4,1)S(1)}, s32[]{:S(2)}) async-start(s8[8388608]{0:T(1024)(128)(4,1)} %bitcast.48), calls=%async_computation.1 | async-start | bytes 8388608
  10.2 21.2 %collective-permute-start = (bf16[64,2048]{1,0:T(8,128)(2,1)S(1)}, bf16[64,2048]{1,0:T(8,128)(2,1)S(1)}, u32[]{:S(2)}, u32[]{:S(2)}) collective-permute-start(bf16[64,2048]{1,0:T(8,128)(2,1)S(1)} %fusion.128), channel_id=1, source_target_pairs={{0,1},{1,2},{2,3},{3,0},{4,5},{5,6},{6,7},{7,4},{8,9},{9,10},{10,1... | collective-permute-start | bytes 786440 | tf_op jit(solution)/shard_map/ppermute | solution.py:26
  10.8 20.7 %collective-permute-start.1 = (bf16[64,2048]{1,0:T(8,128)(2,1)S(1)}, bf16[64,2048]{1,0:T(8,128)(2,1)S(1)}, u32[]{:S(2)}, u32[]{:S(2)}) collective-permute-start(bf16[64,2048]{1,0:T(8,128)(2,1)S(1)} %fusion.128), channel_id=1, source_target_pairs={{0,2},{1,3},{2,0},{3,1},{4,6},{5,7},{6,4},{7,5},{8,10},{9,11},{10,... | collective-permute-start | bytes 786440 | tf_op jit(solution)/shard_map/ppermute | solution.py:26
  13.3 18.2 %collective-permute-start.2 = (bf16[64,2048]{1,0:T(8,128)(2,1)S(1)}, bf16[64,2048]{1,0:T(8,128)(2,1)S(1)}, u32[]{:S(2)}, u32[]{:S(2)}) collective-permute-start(bf16[64,2048]{1,0:T(8,128)(2,1)S(1)} %fusion.128), channel_id=1, source_target_pairs={{0,3},{1,0},{2,1},{3,2},{4,7},{5,4},{6,5},{7,6},{8,11},{9,8},{10,9... | collective-permute-start | bytes 786440 | tf_op jit(solution)/shard_map/ppermute | solution.py:26
  20.3 6.6 %slice-start.1 = ((s8[8388608]{0:T(1024)(128)(4,1)}), s8[4194304]{0:T(1024)(128)(4,1)S(1)}, s32[]{:S(2)}) async-start(s8[8388608]{0:T(1024)(128)(4,1)} %bitcast.48), calls=%async_computation.2 | async-start | bytes 8388608
  26.9 8.7 %copy-start.8 = (bf16[2,2048,2048]{2,1,0:T(8,128)(2,1)S(1)}, bf16[2,2048,2048]{2,1,0:T(8,128)(2,1)}, u32[]{:S(2)}) copy-start(bf16[2,2048,2048]{2,1,0:T(8,128)(2,1)} %param.14) | copy-start | bytes 50331652
  129.2 56.0 %copy-start.2 = (bf16[2048,1024]{1,0:T(8,128)(2,1)S(1)}, bf16[2048,1024]{1,0:T(8,128)(2,1)}, u32[]{:S(2)}) copy-start(bf16[2048,1024]{1,0:T(8,128)(2,1)} %get-tuple-element.10) | copy-start | bytes 12582916
  185.2 2.5 copy-start.10
  188.5 35.9 %slice-start.2 = ((s8[16777216]{0:T(1024)(128)(4,1)}), s8[4194304]{0:T(1024)(128)(4,1)S(1)}, s32[]{:S(2)}) async-start(s8[16777216]{0:T(1024)(128)(4,1)} %bitcast.68), calls=%async_computation.3 | async-start | bytes 8388608
  189.2 35.2 %slice-start.3 = ((s8[16777216]{0:T(1024)(128)(4,1)}), s8[4194304]{0:T(1024)(128)(4,1)S(1)}, s32[]{:S(2)}) async-start(s8[16777216]{0:T(1024)(128)(4,1)} %bitcast.68), calls=%async_computation.4 | async-start | bytes 8388608
  190.0 34.4 %slice-start.4 = ((s8[16777216]{0:T(1024)(128)(4,1)}), s8[4194304]{0:T(1024)(128)(4,1)S(1)}, s32[]{:S(2)}) async-start(s8[16777216]{0:T(1024)(128)(4,1)} %bitcast.68), calls=%async_computation.5 | async-start | bytes 8388608
  190.0 34.4 %slice-start.5 = ((s8[16777216]{0:T(1024)(128)(4,1)}), s8[4194304]{0:T(1024)(128)(4,1)S(1)}, s32[]{:S(2)}) async-start(s8[16777216]{0:T(1024)(128)(4,1)} %bitcast.68), calls=%async_computation.6 | async-start | bytes 8388608
  196.5 7.9 %collective-permute-start.3 = (bf16[64,2048]{1,0:T(8,128)(2,1)S(1)}, bf16[64,2048]{1,0:T(8,128)(2,1)S(1)}, u32[]{:S(2)}, u32[]{:S(2)}) collective-permute-start(bf16[64,2048]{1,0:T(8,128)(2,1)S(1)} %get-tuple-element.14), channel_id=1, source_target_pairs={{0,3},{1,0},{2,1},{3,2},{4,7},{5,4},{6,5},{7,6},{8,11},{9,8},{10,9... | collective-permute-start | bytes 786440 | tf_op jit(solution)/shard_map/ppermute | solution.py:26
  197.7 13.2 %collective-permute-start.4 = (bf16[64,2048]{1,0:T(8,128)(2,1)S(1)}, bf16[64,2048]{1,0:T(8,128)(2,1)S(1)}, u32[]{:S(2)}, u32[]{:S(2)}) collective-permute-start(bf16[64,2048]{1,0:T(8,128)(2,1)S(1)} %get-tuple-element.16), channel_id=1, source_target_pairs={{0,2},{1,3},{2,0},{3,1},{4,6},{5,7},{6,4},{7,5},{8,10},{9,11},{10,... | collective-permute-start | bytes 786440 | tf_op jit(solution)/shard_map/ppermute | solution.py:26
  198.4 12.5 %collective-permute-start.5 = (bf16[64,2048]{1,0:T(8,128)(2,1)S(1)}, bf16[64,2048]{1,0:T(8,128)(2,1)S(1)}, u32[]{:S(2)}, u32[]{:S(2)}) collective-permute-start(bf16[64,2048]{1,0:T(8,128)(2,1)S(1)} %get-tuple-element.15), channel_id=1, source_target_pairs={{0,1},{1,2},{2,3},{3,0},{4,5},{5,6},{6,7},{7,4},{8,9},{9,10},{10,1... | collective-permute-start | bytes 786440 | tf_op jit(solution)/shard_map/ppermute | solution.py:26
  211.3 15.5 %copy-start.1 = (bf16[2048,1024]{1,0:T(8,128)(2,1)S(1)}, bf16[2048,1024]{1,0:T(8,128)(2,1)}, u32[]{:S(2)}) copy-start(bf16[2048,1024]{1,0:T(8,128)(2,1)} %get-tuple-element.7) | copy-start | bytes 12582916
  211.3 8.0 %collective-permute-start.6 = (bf16[64,2048]{1,0:T(8,128)(2,1)S(1)}, bf16[64,2048]{1,0:T(8,128)(2,1)S(1)}, u32[]{:S(2)}, u32[]{:S(2)}) collective-permute-start(bf16[64,2048]{1,0:T(8,128)(2,1)S(1)} %multiply_convert_fusion.16), channel_id=1, source_target_pairs={{0,1},{1,2},{2,3},{3,0},{4,5},{5,6},{6,7},{7,4},{8,9},{9,10},{10,1... | collective-permute-start | bytes 786440 | tf_op jit(solution)/shard_map/ppermute | solution.py:26
  211.4 9.2 %collective-permute-start.7 = (bf16[64,2048]{1,0:T(8,128)(2,1)S(1)}, bf16[64,2048]{1,0:T(8,128)(2,1)S(1)}, u32[]{:S(2)}, u32[]{:S(2)}) collective-permute-start(bf16[64,2048]{1,0:T(8,128)(2,1)S(1)} %multiply_convert_fusion.16), channel_id=1, source_target_pairs={{0,2},{1,3},{2,0},{3,1},{4,6},{5,7},{6,4},{7,5},{8,10},{9,11},{10,... | collective-permute-start | bytes 786440 | tf_op jit(solution)/shard_map/ppermute | solution.py:26
  212.7 11.7 %collective-permute-start.8 = (bf16[64,2048]{1,0:T(8,128)(2,1)S(1)}, bf16[64,2048]{1,0:T(8,128)(2,1)S(1)}, u32[]{:S(2)}, u32[]{:S(2)}) collective-permute-start(bf16[64,2048]{1,0:T(8,128)(2,1)S(1)} %multiply_convert_fusion.16), channel_id=1, source_target_pairs={{0,3},{1,0},{2,1},{3,2},{4,7},{5,4},{6,5},{7,6},{8,11},{9,8},{10,9... | collective-permute-start | bytes 786440 | tf_op jit(solution)/shard_map/ppermute | solution.py:26
  232.4 56.1 %copy-start = (bf16[2048,1024]{1,0:T(8,128)(2,1)S(1)}, bf16[2048,1024]{1,0:T(8,128)(2,1)}, u32[]{:S(2)}) copy-start(bf16[2048,1024]{1,0:T(8,128)(2,1)} %get-tuple-element.9) | copy-start | bytes 12582916
  288.4 2.5 copy-start.9
  293.2 8.4 %copy-start.6 = (bf16[2048]{0:T(1024)(128)(2,1)S(1)}, bf16[2048]{0:T(1024)(128)(2,1)}, u32[]{:S(2)}) copy-start(bf16[2048]{0:T(1024)(128)(2,1)} %param.19) | copy-start | bytes 12292
  299.0 9.2 %collective-permute-start.10 = (bf16[64,2048]{1,0:T(8,128)(2,1)S(1)}, bf16[64,2048]{1,0:T(8,128)(2,1)S(1)}, u32[]{:S(2)}, u32[]{:S(2)}) collective-permute-start(bf16[64,2048]{1,0:T(8,128)(2,1)S(1)} %get-tuple-element.13), channel_id=1, source_target_pairs={{0,2},{1,3},{2,0},{3,1},{4,6},{5,7},{6,4},{7,5},{8,10},{9,11},{10,... | collective-permute-start | bytes 786440 | tf_op jit(solution)/shard_map/ppermute | solution.py:26
  299.8 14.0 %collective-permute-start.11 = (bf16[64,2048]{1,0:T(8,128)(2,1)S(1)}, bf16[64,2048]{1,0:T(8,128)(2,1)S(1)}, u32[]{:S(2)}, u32[]{:S(2)}) collective-permute-start(bf16[64,2048]{1,0:T(8,128)(2,1)S(1)} %get-tuple-element.12), channel_id=1, source_target_pairs={{0,1},{1,2},{2,3},{3,0},{4,5},{5,6},{6,7},{7,4},{8,9},{9,10},{10,1... | collective-permute-start | bytes 786440 | tf_op jit(solution)/shard_map/ppermute | solution.py:26
  301.1 12.8 %collective-permute-start.9 = (bf16[64,2048]{1,0:T(8,128)(2,1)S(1)}, bf16[64,2048]{1,0:T(8,128)(2,1)S(1)}, u32[]{:S(2)}, u32[]{:S(2)}) collective-permute-start(bf16[64,2048]{1,0:T(8,128)(2,1)S(1)} %get-tuple-element.11), channel_id=1, source_target_pairs={{0,3},{1,0},{2,1},{3,2},{4,7},{5,4},{6,5},{7,6},{8,11},{9,8},{10,9... | collective-permute-start | bytes 786440 | tf_op jit(solution)/shard_map/ppermute | solution.py:26
Sparse Core Ops, SparseCore 0:
  10.2 118.9 all-gather.1
where the time goes:
time: 322 us
  waiting for transfers between devices  121 us (38%)
  Pallas kernels  112 us (35%)
  matrix products  31.5 us (10%)
  local copies, waits for them, and re-layouts  16.9 us (5%)
  other arithmetic  15 us (5%)
  between operations  13.7 us (4%)
  starting transfers between devices  11.8 us (4%)
    pallas_call x2, Pallas kernels, attend(): pl.pallas_call(functools.partial(attend_kernel, rows), grid=(positions //...  112 us
    all_gather x1, waiting for transfers between devices, per_device(): lax.all_gather(unit_rows(source).astype(jnp.bfloat16), ('sp', 'tp'), axis...  85.9 us
    ppermute x12, waiting for transfers between devices, shifted(): lax.ppermute(block, 'tp', [(i, (i + shift) % size) for i in range(size)])  35 us
    dot_general x2, matrix products, per_device(): jnp.dot(jnp.concatenate(attended, axis=1), out_w[layer], preferred_elemen...  12.1 us
    ppermute x12, starting transfers between devices, shifted(): lax.ppermute(block, 'tp', [(i, (i + shift) % size) for i in range(size)])  11.8 us
    dot_general x8, matrix products, per_device(): jnp.dot(own, value_w[layer][:, columns], preferred_element_type=jnp.float32)  8.61 us
  transfers between devices with their start and end apart: 13, of which 8 were waited for; matrix products, arithmetic and copies ran while one was open for 7% of the time, Pallas kernels for 0%

commit v1 on v0

--- a/solution.py
+++ b/solution.py
@@ -14,11 +14,591 @@
 CHUNK = 512
 ROWS = 512
 LOG2E = math.log2(math.e)
+MESH = pl.DeviceIdType.MESH
+MIB = 1024 * 1024
+HBM = pl.BlockSpec(memory_space=pl.ANY)
+VMEM = pl.BlockSpec(memory_space=pltpu.VMEM)
+SMEM = pl.BlockSpec(memory_space=pltpu.SMEM)
 
 
 def unit_rows(matrix):
     values = matrix.astype(jnp.float32)
     return values * lax.rsqrt(jnp.mean(values * values, axis=-1, keepdims=True) + EPS)
+
+
+class Place:
+    def __init__(self):
+        sp, tp = lax.axis_index("sp"), lax.axis_index("tp")
+        self.z, self.y = sp // 2, sp % 2
+        self.x, self.core = tp // 2, tp % 2
+        self.up, self.down = (self.z + 1) % 4, (self.z + 3) % 4
+        self.far = (self.z + 2) % 4
+        self.ox, self.oy, self.other = 1 - self.x, 1 - self.y, 1 - self.core
+
+    def at(self, z=None, y=None, x=None, core=None):
+        z = self.z if z is None else z
+        y = self.y if y is None else y
+        x = self.x if x is None else x
+        core = self.core if core is None else core
+        return (z * 2 + y, x * 2 + core)
+
+
+class Copies:
+    def __init__(self, send_sems, recv_sems):
+        self.send_sems, self.recv_sems = send_sems, recv_sems
+        self.index, self.sent = {}, []
+
+    def _make(self, name, ref, target, dst=None):
+        k = self.index.setdefault(name, len(self.index))
+        return pltpu.make_async_remote_copy(
+            src_ref=ref,
+            dst_ref=ref if dst is None else dst,
+            send_sem=self.send_sems.at[k],
+            recv_sem=self.recv_sems.at[k],
+            device_id=target,
+            device_id_type=MESH,
+        )
+
+    def start(self, name, src, target, dst=None):
+        self._make(name, src(), target, dst and dst()).start()
+        self.sent.append((name, src, target, dst))
+
+    def arrived(self, name, ref, source):
+        self._make(name, ref, source).wait_recv()
+
+    def drain(self):
+        for name, src, target, dst in self.sent:
+            self._make(name, src(), target, dst and dst()).wait_send()
+
+
+def greet(targets):
+    barrier = pltpu.get_barrier_semaphore()
+    for target in targets:
+        pl.semaphore_signal(barrier, inc=1, device_id=target, device_id_type=MESH)
+    pl.semaphore_wait(barrier, len(targets))
+
+
+def gather_kernel(
+    own_ref, rows_ref, key_ref, value_ref, gain_ref,
+    kv_ref, normed_ref,
+    blocks, normed, weights, stage, send_sems, recv_sems, local_sems, weight_sems, out_sems,
+):
+    me = Place()
+    z, y, x, core = me.z, me.y, me.x, me.core
+    side = weights.shape[1] // 4
+    steps = blocks.shape[0]
+
+    def plane(c, zz):
+        return blocks.at[c * 4 + zz]
+
+    def column(c, yy, xx):
+        return blocks.at[8 + c * 4 + yy * 2 + xx]
+
+    loads = []
+    for c in range(2):
+        loads.append((own_ref.at[c], plane(c, z).at[y, x, core]))
+        loads.append((own_ref.at[2 + c], column(c, y, x).at[z // 2, z % 2, core]))
+        loads.append((rows_ref.at[c], normed.at[c, y, x, core]))
+    loads = [
+        pltpu.make_async_copy(src, dst, local_sems.at[k]) for k, (src, dst) in enumerate(loads)
+    ]
+    for copy in loads:
+        copy.start()
+    fetches = []
+    for layer in range(2):
+        for part, ref in enumerate((key_ref, value_ref)):
+            n = 2 * layer + part
+            fetches.append(
+                pltpu.make_async_copy(
+                    ref.at[layer, :, pl.ds(pl.multiple_of(y * side, side), side)],
+                    weights.at[:, pl.ds(n * side, side)],
+                    weight_sems.at[n],
+                )
+            )
+    for copy in fetches:
+        copy.start()
+    greet([me.at(x=me.ox), me.at(y=me.oy), me.at(z=me.up), me.at(z=me.down), me.at(core=me.other)])
+    for copy in loads:
+        copy.wait()
+
+    net = Copies(send_sems, recv_sems)
+    sibling, xmate, ymate = me.at(core=me.other), me.at(x=me.ox), me.at(y=me.oy)
+    above, below = me.at(z=me.up), me.at(z=me.down)
+
+    def share(name, mine):
+        net.start(name + "d", lambda: mine(core), sibling)
+
+    def shared(name, mine):
+        net.arrived(name + "d", mine(me.other), sibling)
+
+    a_own = [lambda k, c=c: plane(c, z).at[y, x, k] for c in range(2)]
+    a_one = [lambda k: plane(0, z).at[y, me.ox, k], lambda k: plane(1, z).at[me.oy, x, k]]
+    a_two = [lambda k: plane(0, z).at[me.oy, :, k], lambda k: plane(1, z).at[:, me.ox, k]]
+    a_have = [lambda k: plane(0, z).at[y, :, k], lambda k: plane(1, z).at[:, x, k]]
+    a_all = [lambda k, c=c: plane(c, z).at[:, :, k] for c in range(2)]
+    a_down = [lambda k, c=c: plane(c, me.down).at[:, :, k] for c in range(2)]
+    a_up = [lambda k, c=c: plane(c, me.up).at[:, :, k] for c in range(2)]
+    a_far = [lambda k, c=c: plane(c, me.far).at[:, :, k] for c in range(2)]
+    b_own = [lambda k, c=c: column(c, y, x).at[z // 2, z % 2, k] for c in range(2)]
+    b_down = [lambda k, c=c: column(c, y, x).at[me.down // 2, me.down % 2, k] for c in range(2)]
+    b_up = [lambda k, c=c: column(c, y, x).at[me.up // 2, me.up % 2, k] for c in range(2)]
+    b_far = [lambda k, c=c: column(c, y, x).at[me.far // 2, me.far % 2, k] for c in range(2)]
+    b_all = [lambda k, c=c: column(c, y, x).at[:, :, k] for c in range(2)]
+    b_one = [lambda k: column(0, me.oy, x).at[:, :, k], lambda k: column(1, y, me.ox).at[:, :, k]]
+    b_two = [lambda k: column(0, y, me.ox).at[:, :, k], lambda k: column(1, me.oy, x).at[:, :, k]]
+    b_last = [lambda k, c=c: column(c, me.oy, me.ox).at[:, :, k] for c in range(2)]
+    t_own = [lambda k, c=c: normed.at[c, y, x, k] for c in range(2)]
+    t_one = [lambda k: normed.at[0, y, me.ox, k], lambda k: normed.at[1, me.oy, x, k]]
+    t_two = [lambda k: normed.at[0, me.oy, :, k], lambda k: normed.at[1, :, me.ox, k]]
+    t_have = [lambda k: normed.at[0, y, :, k], lambda k: normed.at[1, :, x, k]]
+    first = [xmate, ymate]
+    second = [ymate, xmate]
+
+    for c in range(2):
+        net.start(f"a{c}1", lambda f=a_own[c]: f(core), first[c])
+    for c in range(2):
+        net.start(f"b{c}u", lambda f=b_own[c]: f(core), above)
+        net.start(f"b{c}w", lambda f=b_own[c]: f(core), below)
+    for c in range(2):
+        net.start(f"t{c}1", lambda f=t_own[c]: f(core), first[c])
+        share(f"b{c}0", b_own[c])
+        share(f"a{c}0", a_own[c])
+        share(f"t{c}0", t_own[c])
+
+    def scale(n):
+        fetches[n].wait()
+        columns = pl.ds(n * side, side)
+
+        def body(i, carry):
+            block = pl.ds(i * 256, 256)
+            weights[block, columns] = (
+                weights[block, columns].astype(jnp.float32) * gain_ref[n // 2, block, :]
+            ).astype(jnp.bfloat16)
+            return carry
+
+        lax.fori_loop(0, weights.shape[0] // 256, body, 0)
+
+    scale(0)
+    for c in range(2):
+        net.arrived(f"a{c}1", a_one[c](core), first[c])
+        net.start(f"a{c}2", lambda f=a_have[c]: f(core), second[c])
+        share(f"a{c}1", a_one[c])
+    scale(1)
+    for c in range(2):
+        net.arrived(f"b{c}u", b_down[c](core), below)
+        if c == 0:
+            net.start(f"b{c}f", lambda f=b_down[c]: f(core), above)
+        share(f"b{c}1", b_down[c])
+        net.arrived(f"b{c}w", b_up[c](core), above)
+        if c == 1:
+            net.start(f"b{c}f", lambda f=b_up[c]: f(core), below)
+        share(f"b{c}2", b_up[c])
+    for c in range(2):
+        net.arrived(f"t{c}1", t_one[c](core), first[c])
+        net.start(f"t{c}2", lambda f=t_have[c]: f(core), second[c])
+        share(f"t{c}1", t_one[c])
+    scale(2)
+    for c in range(2):
+        net.arrived(f"b{c}f", b_far[c](core), below if c == 0 else above)
+        net.start(f"b{c}y", lambda f=b_all[c]: f(core), second[c])
+        net.start(f"b{c}x", lambda f=b_all[c]: f(core), first[c])
+        share(f"b{c}3", b_far[c])
+    scale(3)
+
+    def on_columns():
+        for c in range(2):
+            for k, part in enumerate((b_own, b_down, b_up, b_far)):
+                shared(f"b{c}{k}", part[c])
+
+    def on_planes():
+        for c in range(2):
+            net.arrived(f"a{c}2", a_two[c](core), second[c])
+            net.start(f"a{c}u", lambda f=a_all[c]: f(core), above)
+            net.start(f"a{c}w", lambda f=a_all[c]: f(core), below)
+            share(f"a{c}2", a_two[c])
+
+    def on_planes_shared():
+        for c in range(2):
+            for k, part in enumerate((a_own, a_one, a_two)):
+                shared(f"a{c}{k}", part[c])
+
+    def on_rows():
+        for c in range(2):
+            net.arrived(f"t{c}2", t_two[c](core), second[c])
+            share(f"t{c}2", t_two[c])
+
+    def on_next(c):
+        net.arrived(f"a{c}u", a_down[c](core), below)
+        if c == 0:
+            net.start(f"a{c}f", lambda f=a_down[c]: f(core), above)
+        share(f"a{c}3", a_down[c])
+        net.arrived(f"a{c}w", a_up[c](core), above)
+        if c == 1:
+            net.start(f"a{c}f", lambda f=a_up[c]: f(core), below)
+        share(f"a{c}4", a_up[c])
+        shared(f"a{c}3", a_down[c])
+        shared(f"a{c}4", a_up[c])
+
+    def on_one():
+        for c in range(2):
+            net.arrived(f"b{c}y", b_one[c](core), second[c])
+            net.start(f"b{c}z", lambda f=b_one[c]: f(core), first[c])
+            share(f"b{c}4", b_one[c])
+        for c in range(2):
+            shared(f"b{c}4", b_one[c])
+
+    def on_two():
+        for c in range(2):
+            net.arrived(f"b{c}x", b_two[c](core), first[c])
+            share(f"b{c}5", b_two[c])
+        for c in range(2):
+            shared(f"b{c}5", b_two[c])
+
+    def on_far():
+        for c in range(2):
+            net.arrived(f"a{c}f", a_far[c](core), below if c == 0 else above)
+            share(f"a{c}5", a_far[c])
+        for c in range(2):
+            shared(f"a{c}5", a_far[c])
+
+    def on_last():
+        for c in range(2):
+            net.arrived(f"b{c}z", b_last[c](core), first[c])
+            share(f"b{c}6", b_last[c])
+        for c in range(2):
+            shared(f"b{c}6", b_last[c])
+
+    handlers = {
+        0: [on_columns],
+        1: [on_planes],
+        2: [on_planes_shared],
+        3: [on_rows],
+        4: [lambda: on_next(0)],
+        6: [on_one],
+        8: [lambda: on_next(1)],
+        10: [on_two],
+        12: [on_far],
+        14: [on_last],
+    }
+    order = [
+        8 + y * 2 + x, 12 + y * 2 + x, z, 4 + z,
+        me.down, me.up, 8 + me.oy * 2 + x, 12 + y * 2 + me.ox,
+        4 + me.down, 4 + me.up, 8 + y * 2 + me.ox, 12 + me.oy * 2 + x,
+        me.far, 4 + me.far, 8 + me.oy * 2 + me.ox, 12 + me.oy * 2 + me.ox,
+    ]
+
+    def leave(s, slot):
+        return pltpu.make_async_copy(stage.at[slot], kv_ref.at[s], out_sems.at[slot])
+
+    count = math.prod(blocks.shape[1:5])
+
+    def step(s, carry):
+        for k, calls in handlers.items():
+
+            @pl.when(s == k)
+            def _():
+                for call in calls:
+                    call()
+
+        which = order[0]
+        for k in range(1, steps):
+            which = jnp.where(s == k, order[k], which)
+        slot = s % 2
+
+        @pl.when(s >= 2)
+        def _():
+            leave(s - 2, slot).wait()
+
+        block = blocks[which].reshape(count, blocks.shape[5])
+        for n in range(4):
+            stage[slot, :, n * side : (n + 1) * side] = jnp.dot(
+                block, weights[:, n * side : (n + 1) * side], preferred_element_type=jnp.float32
+            ).astype(jnp.bfloat16)
+        leave(s, slot).start()
+        return carry
+
+    lax.fori_loop(0, steps, step, 0)
+    for c in range(2):
+        for k, part in enumerate((t_own, t_one, t_two)):
+            shared(f"t{c}{k}", part[c])
+    final = pltpu.make_async_copy(normed, normed_ref, local_sems.at[0])
+    final.start()
+    leave(steps - 2, 0).wait()
+    leave(steps - 1, 1).wait()
+    net.drain()
+    final.wait()
+
+
+def gather_and_project(own, rows, key_w, value_w, gain):
+    width = own.shape[1]
+    piece, share = own.shape[0] // 4, rows.shape[0] // 2
+    copies = 58
+    return pl.pallas_call(
+        gather_kernel,
+        out_shape=(
+            jax.ShapeDtypeStruct((16, 8 * piece, 4 * HEAD_DIM), jnp.bfloat16),
+            jax.ShapeDtypeStruct((2, 2, 2, 2, share, width), jnp.bfloat16),
+        ),
+        in_specs=[HBM, HBM, HBM, HBM, VMEM],
+        out_specs=(HBM, HBM),
+        scratch_shapes=[
+            pltpu.VMEM((16, 2, 2, 2, piece, width), jnp.bfloat16),
+            pltpu.VMEM((2, 2, 2, 2, share, width), jnp.bfloat16),
+            pltpu.VMEM((width, 4 * HEAD_DIM), jnp.bfloat16),
+            pltpu.VMEM((2, 8 * piece, 4 * HEAD_DIM), jnp.bfloat16),
+            pltpu.SemaphoreType.DMA((copies,)),
+            pltpu.SemaphoreType.DMA((copies,)),
+            pltpu.SemaphoreType.DMA((6,)),
+            pltpu.SemaphoreType.DMA((4,)),
+            pltpu.SemaphoreType.DMA((2,)),
+        ],
+        compiler_params=pltpu.CompilerParams(
+            collective_id=0, has_side_effects=True, vmem_limit_bytes=48 * MIB
+        ),
+    )(
+        own.reshape(4, piece, width),
+        rows.reshape(2, share, width),
+        key_w,
+        value_w,
+        gain,
+    )
+
+
+def attend_kernel(
+    layer, group, normed_ref, query_ref, out_ref, kv_ref, temp_ref, partial_ref,
+    rows, query_w, out_w, kv, query, total, tops, sums, sems,
+):
+    y = lax.axis_index("sp") % 2
+    count = rows.shape[0]
+    wide = group * HEAD_DIM
+    chunks = kv.shape[0]
+    span = pl.ds(pl.multiple_of(y * wide, wide), wide)
+    fetch = [
+        pltpu.make_async_copy(normed_ref, rows, sems.at[0]),
+        pltpu.make_async_copy(query_ref.at[layer, :, span], query_w, sems.at[1]),
+    ]
+    held = [
+        pltpu.make_async_copy(
+            kv_ref.at[j, :, pl.ds(layer * 2 * HEAD_DIM, 2 * HEAD_DIM)], kv.at[j], sems.at[3 + j]
+        )
+        for j in range(chunks)
+    ]
+    final = pltpu.make_async_copy(out_ref.at[layer, span, :], out_w, sems.at[2])
+    for copy in fetch + held + [final]:
+        copy.start()
+    for copy in fetch:
+        copy.wait()
+    for head in range(group):
+        scale = temp_ref[layer, y * group + head] * (HEAD_DIM ** (-0.5) * LOG2E)
+        query[head] = (
+            jnp.dot(
+                rows[...],
+                query_w[:, head * HEAD_DIM : (head + 1) * HEAD_DIM],
+                preferred_element_type=jnp.float32,
+            )
+            * scale
+        ).astype(jnp.bfloat16)
+    total[...] = jnp.zeros_like(total)
+    sums[...] = jnp.zeros_like(sums)
+    tops[...] = jnp.full_like(tops, FLOOR)
+    for copy in held:
+        copy.wait()
+
+    def step(j, carry):
+        for head in range(group):
+            scores = lax.dot_general(
+                query[head],
+                kv[j, :, :HEAD_DIM],
+                (((1,), (1,)), ((), ())),
+                preferred_element_type=jnp.float32,
+            )
+            old_top = tops[head, :, :1]
+            new_top = jnp.maximum(old_top, jnp.max(scores, axis=-1, keepdims=True))
+            shrink = jnp.exp2(old_top - new_top)
+            expo = jnp.exp2(scores - new_top)
+            tops[head] = jnp.broadcast_to(new_top, tops.shape[1:])
+            new_sum = sums[head, :, :1] * shrink + jnp.sum(expo, axis=-1, keepdims=True)
+            sums[head] = jnp.broadcast_to(new_sum, sums.shape[1:])
+            total[head] = total[head] * shrink + jnp.dot(
+                expo.astype(jnp.bfloat16), kv[j, :, HEAD_DIM:], preferred_element_type=jnp.float32
+            )
+        return carry
+
+    lax.fori_loop(0, chunks, step, 0)
+    final.wait()
+    attended = jnp.concatenate(
+        [(total[head] / sums[head, :, :1]).astype(jnp.bfloat16) for head in range(group)], axis=1
+    )
+    columns = partial_ref.shape[1]
+    for start in range(0, columns, HEAD_DIM):
+        block = slice(start, start + HEAD_DIM)
+        partial_ref[:, block] = jnp.dot(
+            attended, out_w[:, block], preferred_element_type=jnp.float32
+        ).astype(jnp.bfloat16)
+
+
+def attend_layer(layer, group, normed, query_w, out_w, kv, head_temp, chunk=1024):
+    count, width = normed.shape
+    positions = kv.shape[0] * kv.shape[1]
+    chunk = math.gcd(chunk, positions)
+    kv = kv.reshape(positions // chunk, chunk, kv.shape[2])
+    wide = group * HEAD_DIM
+    return pl.pallas_call(
+        functools.partial(attend_kernel, layer, group),
+        out_shape=jax.ShapeDtypeStruct((count, width), jnp.bfloat16),
+        in_specs=[HBM, HBM, HBM, HBM, SMEM],
+        out_specs=VMEM,
+        scratch_shapes=[
+            pltpu.VMEM((count, width), jnp.bfloat16),
+            pltpu.VMEM((width, wide), jnp.bfloat16),
+            pltpu.VMEM((wide, width), jnp.bfloat16),
+            pltpu.VMEM((positions // chunk, chunk, 2 * HEAD_DIM), jnp.bfloat16),
+            pltpu.VMEM((group, count, HEAD_DIM), jnp.bfloat16),
+            pltpu.VMEM((group, count, HEAD_DIM), jnp.float32),
+            pltpu.VMEM((group, count, 128), jnp.float32),
+            pltpu.VMEM((group, count, 128), jnp.float32),
+            pltpu.SemaphoreType.DMA((3 + positions // chunk,)),
+        ],
+        compiler_params=pltpu.CompilerParams(vmem_limit_bytes=52 * MIB),
+        cost_estimate=pl.CostEstimate(
+            flops=4 * count * width * wide + 4 * count * positions * wide,
+            bytes_accessed=4 * positions * HEAD_DIM + 4 * width * wide,
+            transcendentals=group * count * positions,
+        ),
+    )(normed, query_w, out_w, kv, head_temp)
+
+
+def fold_kernel(last, partial_ref, state_ref, gain_ref, *refs):
+    if last:
+        result_ref, *refs = refs
+    else:
+        state_out, normed_ref, *refs = refs
+    from_core, sums, from_first, relay, from_second, normed, send_sems, recv_sems, local_sem = refs
+    me = Place()
+    y, x, core = me.y, me.x, me.core
+    sibling, xmate, ymate = me.at(core=me.other), me.at(x=me.ox), me.at(y=me.oy)
+    first, second = [xmate, ymate], [ymate, xmate]
+    greet([sibling, xmate, ymate])
+    net = Copies(send_sems, recv_sems)
+    sides = [[me.oy, y], [me.ox, x]]
+
+    def piece(ref, c, k, who):
+        return ref.at[c, sides[c][k], :, who] if c == 0 else ref.at[c, :, sides[c][k], who]
+
+    for k in range(2):
+        for c in range(2):
+            net.start(
+                f"c{c}{k}",
+                lambda c=c, k=k: piece(partial_ref, c, k, me.other),
+                sibling,
+                lambda c=c, k=k: from_core.at[c, k],
+            )
+    for k in range(2):
+        for c in range(2):
+            net.arrived(f"c{c}{k}", from_core.at[c, k], sibling)
+            mine = piece(partial_ref, c, k, core)[...]
+            sums[c, k] = (
+                mine.astype(jnp.float32) + from_core[c, k].astype(jnp.float32)
+            ).astype(jnp.bfloat16)
+            if k == 0:
+                net.start(
+                    f"p{c}",
+                    lambda c=c: sums.at[c, 0],
+                    second[c],
+                    lambda c=c: from_first.at[c],
+                )
+    spots = [(x, me.ox), (y, me.oy)]
+    for c in range(2):
+        near, far = spots[c]
+        net.arrived(f"p{c}", from_first.at[c], second[c])
+        relay[c] = (
+            sums[c, 1, far].astype(jnp.float32) + from_first[c, far].astype(jnp.float32)
+        ).astype(jnp.bfloat16)
+        net.start(f"q{c}", lambda c=c: relay.at[c], first[c], lambda c=c: from_second.at[c])
+    for c in range(2):
+        near, far = spots[c]
+        partly = sums[c, 1, near].astype(jnp.float32) + from_first[c, near].astype(jnp.float32)
+        net.arrived(f"q{c}", from_second.at[c], first[c])
+        state = state_ref[c] + (partly + from_second[c].astype(jnp.float32))
+        rows = unit_rows(state) * gain_ref[...]
+        if last:
+            result_ref[c] = rows
+        else:
+            state_out[c] = state
+            normed[c, y, x, core] = rows.astype(jnp.bfloat16)
+            net.start(f"t{c}", lambda c=c: normed.at[c, y, x, core], first[c])
+            net.start(f"s{c}0", lambda c=c: normed.at[c, y, x, core], sibling)
+    if not last:
+        one = [lambda k: normed.at[0, y, me.ox, k], lambda k: normed.at[1, me.oy, x, k]]
+        two = [lambda k: normed.at[0, me.oy, :, k], lambda k: normed.at[1, :, me.ox, k]]
+        have = [lambda k: normed.at[0, y, :, k], lambda k: normed.at[1, :, x, k]]
+        for c in range(2):
+            net.arrived(f"t{c}", one[c](core), first[c])
+            net.start(f"u{c}", lambda c=c: have[c](core), second[c])
+            net.start(f"s{c}1", lambda c=c: one[c](core), sibling)
+        for c in range(2):
+            net.arrived(f"u{c}", two[c](core), second[c])
+            net.start(f"s{c}2", lambda c=c: two[c](core), sibling)
+        for c in range(2):
+            net.arrived(f"s{c}0", normed.at[c, y, x, me.other], sibling)
+            net.arrived(f"s{c}1", one[c](me.other), sibling)
+            net.arrived(f"s{c}2", two[c](me.other), sibling)
+        copy = pltpu.make_async_copy(normed, normed_ref, local_sem)
+        copy.start()
+        copy.wait()
+    net.drain()
+
+
+def fold(last, partial, state, gain):
+    share, width = state.shape[1:]
+    result = jax.ShapeDtypeStruct(state.shape, jnp.float32)
+    normed = jax.ShapeDtypeStruct((2, 2, 2, 2, share, width), jnp.bfloat16)
+    return pl.pallas_call(
+        functools.partial(fold_kernel, last),
+        out_shape=result if last else (result, normed),
+        in_specs=[VMEM, VMEM, VMEM],
+        out_specs=VMEM if last else (VMEM, HBM),
+        scratch_shapes=[
+            pltpu.VMEM((2, 2, 2, share, width), jnp.bfloat16),
+            pltpu.VMEM((2, 2, 2, share, width), jnp.bfloat16),
+            pltpu.VMEM((2, 2, share, width), jnp.bfloat16),
+            pltpu.VMEM((2, share, width), jnp.bfloat16),
+            pltpu.VMEM((2, share, width), jnp.bfloat16),
+            pltpu.VMEM((2, 2, 2, 2, share, width), jnp.bfloat16),
+            pltpu.SemaphoreType.DMA((20,)),
+            pltpu.SemaphoreType.DMA((20,)),
+            pltpu.SemaphoreType.DMA,
+        ],
+        compiler_params=pltpu.CompilerParams(
+            collective_id=2 if last else 1, has_side_effects=True, vmem_limit_bytes=32 * MIB
+        ),
+    )(partial.reshape(2, 2, 2, 2, share, width), state, gain)
+
+
+def on_planes(
+    target, source, target_gain, source_gain, query_w, key_w, value_w, out_w, head_temp, final_gain
+):
+    width = target.shape[1]
+    group = query_w.shape[2] // key_w.shape[2]
+    state = target.astype(jnp.float32)
+    rows = (unit_rows(state) * target_gain[0].astype(jnp.float32)).astype(jnp.bfloat16)
+    kv, normed = gather_and_project(
+        unit_rows(source).astype(jnp.bfloat16),
+        rows,
+        key_w,
+        value_w,
+        source_gain.astype(jnp.float32)[:, :, None],
+    )
+    state = state.reshape(2, -1, width)
+    for layer in range(2):
+        partial = attend_layer(
+            layer, group, normed.reshape(-1, width), query_w, out_w, kv, head_temp
+        )
+        if layer == 0:
+            gain = target_gain[1].astype(jnp.float32).reshape(1, width)
+            state, normed = fold(False, partial, state, gain)
+    gain = final_gain.astype(jnp.float32).reshape(1, width)
+    return fold(True, partial, state, gain).reshape(-1, width)
 
 
 def shifted(block, shift):
@@ -40,7 +620,7 @@
     return mixed
 
 
-def attend_kernel(rows, query_ref, source_ref, mix_ref, total_ref, top_ref, sum_ref):
+def flash_kernel(rows, query_ref, source_ref, mix_ref, total_ref, top_ref, sum_ref):
     step = pl.program_id(0)
     count = query_ref.shape[0]
 
@@ -82,7 +662,7 @@
     chunk = math.gcd(chunk, positions)
     rows = math.gcd(rows, count)
     return pl.pallas_call(
-        functools.partial(attend_kernel, rows),
+        functools.partial(flash_kernel, rows),
         grid=(positions // chunk,),
         out_shape=jax.ShapeDtypeStruct((count, width), jnp.bfloat16),
         in_specs=[
@@ -166,6 +746,10 @@
     return unit_rows(hidden_state) * final_gain.astype(jnp.float32)
 
 
+def fits(mesh):
+    return dict(mesh.shape) == {"sp": 8, "tp": 4}
+
+
 def solution(mesh):
     in_specs = (
         P(("sp", "tp"), None),
@@ -181,5 +765,5 @@
     )
     out_specs = P(("sp", "tp"), None)
     return jax.shard_map(
-        per_device, mesh=mesh, in_specs=in_specs, out_specs=out_specs, check_vma=False
+        on_planes if fits(mesh) else per_device, mesh=mesh, in_specs=in_specs, out_specs=out_specs, check_vma=False
     )

time: 322 us -> 226 us (0.70)
  waiting for transfers between devices: 121 us -> 0 us
  Pallas kernels: 112 us -> 212 us
  matrix products: 31.5 us -> 0 us
  between operations: 13.7 us -> 0.14 us
  starting transfers between devices: 11.8 us -> 0 us
  local copies, waits for them, and re-layouts: 16.9 us -> 7.25 us
  other arithmetic: 15 us -> 6.18 us
    pallas_call x2 -> x5, Pallas kernels: 112 us -> 212 us  [the longest x1 115 us: gather_and_project(): pl.pallas_call(gather_kernel, out_shape=(jax.ShapeDtypeStruct((16, 8 * pi...]
    all_gather x1 -> x0, waiting for transfers between devices: 85.9 us -> none  [per_device(): lax.all_gather(unit_rows(source).astype(jnp.bfloat16), ('sp', 'tp'), axis...]
    ppermute x12 -> x0, waiting for transfers between devices: 35 us -> none  [shifted(): lax.ppermute(block, 'tp', [(i, (i + shift) % size) for i in range(size)])]
    dot_general x20 -> x0, matrix products: 31.5 us -> none  [the longest x2 12.1 us: per_device(): jnp.dot(jnp.concatenate(attended, axis=1), out_w[layer], preferred_elemen...]
    ppermute x12 -> x0, starting transfers between devices: 11.8 us -> none  [shifted(): lax.ppermute(block, 'tp', [(i, (i + shift) % size) for i in range(size)])]
    squeeze x2 -> x0, local copies, waits for them, and re-layouts: 10.4 us -> none  [the longest x1 5.86 us: per_device(): key_w[layer][:, columns]]
    mul x4 -> x0, other arithmetic: 5.91 us -> none  [the longest x1 4.89 us: per_device(): gain * scales[head]]
    concatenate x2 -> x0, other arithmetic: 4.84 us -> none  [per_device(): mix = attend(jnp.concatenate(lifted, axis=0), positions)]
  transfers between devices with their start and end apart: 13 -> 0, of which waited for: 8 -> 0; matrix products, arithmetic and copies ran while one was open for 7% -> 0% of each run, Pallas kernels for 0% -> 0%
where the time goes in v1:
time: 226 us
  Pallas kernels  212 us (94%)
  local copies, waits for them, and re-layouts  7.25 us (3%)
  other arithmetic  6.18 us (3%)
    pallas_call x1, Pallas kernels, gather_and_project(): pl.pallas_call(gather_kernel, out_shape=(jax.ShapeDtypeStruct((16, 8 * pi...  115 us
    pallas_call x2, Pallas kernels, attend_layer(): pl.pallas_call(functools.partial(attend_kernel, layer, group), out_shape=...  52.9 us
    pallas_call x2, Pallas kernels, fold(): pl.pallas_call(functools.partial(fold_kernel, last), out_shape=result if...  44 us
    unnamed x15, local copies, waits for them, and re-layouts  6.61 us

profile of v1, /device:TPU:0, one launch (start us, length us, event | category | flops | bytes accessed | tf_op | source)
XLA Modules:
  0.0 225.6 jit_solution(13524125283317593614)
XLA Ops:
  0.0 0.8 slice_convert_fusion
  0.8 1.1 multiply_reduce_fusion
  1.9 1.1 multiply_convert_fusion
  3.0 0.7 bitcast_convert_fusion
  3.7 0.6 copy.11.gain_ref
  4.4 1.2 fusion
  5.6 1.2 fusion.1
  6.8 0.0 copy-start.4
  6.8 115.2 %shard_map.100 = (bf16[16,256,2048]{2,1,0:T(8,128)(2,1)}, bf16[2,2,2,2,32,2048]{5,4,3,2,1,0:T(8,128)(2,1)S(1)}) custom-call(bf16[4,32,2048]{2,1,0:T(8,128)(2,1)S(1)} %bitcast.19, bf16[2,32,2048]{2,1,0:T(8,128)(2,1)S(1)} %bitcast.21, bf16[2,2048,1024]{2,1,0:T(8,128)(2,1)} %key_ref.1, bf16[2,2048,1024]{2,1,0:T(8,128)(2,1)} %value_ref.1, ...), custom_call_target="tpu_custom_call" | custom-call | tf_op jit(solution)/shard_map/pallas_call | solution.py:336
  122.0 0.0 copy-start.3
  122.0 1.3 copy-done.3
  123.3 0.0 copy-done.4
  123.3 0.0 copy-start.5
  123.3 26.5 %shard_map.101 = bf16[512,2048]{1,0:T(8,128)(2,1)} custom-call(bf16[512,2048]{1,0:T(8,128)(2,1)} %bitcast.18, bf16[2,2048,2048]{2,1,0:T(8,128)(2,1)} %query_ref.3, bf16[2,2048,2048]{2,1,0:T(8,128)(2,1)} %out_ref.3, bf16[4,1024,2048]{2,1,0:T(8,128)(2,1)} %bitcast.23, f32[2,4]{1,0:T(2,128)S(1)} %copy-done.4), custom_call_target="tpu_custom_call" | custom-call | flops 12884901888 | bytes 16777216 | tf_op jit(solution)/shard_map/pallas_call | solution.py:446
  149.8 0.0 copy-done.5
  149.8 0.0 copy-start
  149.9 1.6 copy-done
  151.4 28.3 %shard_map.102 = (f32[2,32,2048]{2,1,0:T(8,128)S(1)}, bf16[2,2,2,2,32,2048]{5,4,3,2,1,0:T(8,128)(2,1)S(1)}) custom-call(bf16[2,2,2,2,32,2048]{5,4,3,2,1,0:T(8,128)(2,1)S(1)} %bitcast.15, f32[2,32,2048]{2,1,0:T(8,128)S(1)} %convert.5.state_ref, f32[1,2048]{1,0:T(1,128)S(1)} %get-tuple-element.13.gain_ref), custom_call_target="tpu_custom_call" | custom-call | tf_op jit(solution)/shard_map/pallas_call | solution.py:556
  179.7 0.0 copy-start.2
  179.7 1.3 copy-done.2
  181.1 0.0 copy-start.6
  181.1 26.5 %shard_map.103 = bf16[512,2048]{1,0:T(8,128)(2,1)} custom-call(bf16[512,2048]{1,0:T(8,128)(2,1)} %bitcast.17, bf16[2,2048,2048]{2,1,0:T(8,128)(2,1)} %query_ref.3, bf16[2,2048,2048]{2,1,0:T(8,128)(2,1)} %out_ref.3, bf16[4,1024,2048]{2,1,0:T(8,128)(2,1)} %bitcast.24, f32[2,4]{1,0:T(2,128)S(1)} %copy-done.4), custom_call_target="tpu_custom_call" | custom-call | flops 12884901888 | bytes 16777216 | tf_op jit(solution)/shard_map/pallas_call | solution.py:446
  207.5 0.0 copy-done.6
  207.6 0.0 copy-start.1
  207.6 1.6 copy-done.1
  209.1 15.7 %shard_map.104 = f32[2,32,2048]{2,1,0:T(8,128)S(1)} custom-call(bf16[2,2,2,2,32,2048]{5,4,3,2,1,0:T(8,128)(2,1)S(1)} %bitcast.16, f32[2,32,2048]{2,1,0:T(8,128)S(1)} %get-tuple-element.12.state_ref, f32[1,2048]{1,0:T(1,128)S(1)} %bitcast.22), custom_call_target="tpu_custom_call" | custom-call | tf_op jit(solution)/shard_map/pallas_call | solution.py:556
  224.8 0.8 copy.13
  (4 shorter events, 0.1 us)
Async XLA Ops:
  6.8 116.5 %copy-start.4 = (f32[2,4]{1,0:T(2,128)S(1)}, f32[2,4]{1,0:T(2,128)}, u32[]{:S(2)}) copy-start(f32[2,4]{1,0:T(2,128)} %temp_ref.3) | copy-start | bytes 100
  122.0 1.3 copy-start.3
  123.3 26.5 %copy-start.5 = (bf16[64,2048]{1,0:T(8,128)(2,1)S(1)}, bf16[64,2048]{1,0:T(8,128)(2,1)}, u32[]{:S(2)}) copy-start(bf16[64,2048]{1,0:T(8,128)(2,1)} %param.10) | copy-start | bytes 786436
  149.8 1.6 copy-start
  179.7 1.3 copy-start.2
  181.1 26.5 %copy-start.6 = (bf16[2048]{0:T(1024)(128)(2,1)S(1)}, bf16[2048]{0:T(1024)(128)(2,1)}, u32[]{:S(2)}) copy-start(bf16[2048]{0:T(1024)(128)(2,1)} %param.19) | copy-start | bytes 12292
  207.6 1.6 copy-start.1

commit v2 on v0

--- a/solution.py
+++ b/solution.py
@@ -13,12 +13,598 @@
 FLOOR = -1e30
 CHUNK = 512
 ROWS = 512
+UNIT = 256
 LOG2E = math.log2(math.e)
+MESH = pl.DeviceIdType.MESH
+MIB = 1024 * 1024
+HBM = pl.BlockSpec(memory_space=pl.ANY)
+VMEM = pl.BlockSpec(memory_space=pltpu.VMEM)
+SMEM = pl.BlockSpec(memory_space=pltpu.SMEM)
 
 
 def unit_rows(matrix):
     values = matrix.astype(jnp.float32)
     return values * lax.rsqrt(jnp.mean(values * values, axis=-1, keepdims=True) + EPS)
+
+
+class Place:
+    def __init__(self):
+        sp, tp = lax.axis_index("sp"), lax.axis_index("tp")
+        self.z, self.y = sp // 2, sp % 2
+        self.x, self.core = tp // 2, tp % 2
+        self.up, self.down = (self.z + 1) % 4, (self.z + 3) % 4
+        self.far = (self.z + 2) % 4
+        self.ox, self.oy, self.other = 1 - self.x, 1 - self.y, 1 - self.core
+
+    def at(self, z=None, y=None, x=None, core=None):
+        z = self.z if z is None else z
+        y = self.y if y is None else y
+        x = self.x if x is None else x
+        core = self.core if core is None else core
+        return (z * 2 + y, x * 2 + core)
+
+
+class Copies:
+    def __init__(self, send_sems, recv_sems):
+        self.send_sems, self.recv_sems = send_sems, recv_sems
+        self.index, self.sent = {}, []
+
+    def _make(self, name, ref, target, dst=None):
+        k = self.index.setdefault(name, len(self.index))
+        return pltpu.make_async_remote_copy(
+            src_ref=ref,
+            dst_ref=ref if dst is None else dst,
+            send_sem=self.send_sems.at[k],
+            recv_sem=self.recv_sems.at[k],
+            device_id=target,
+            device_id_type=MESH,
+        )
+
+    def start(self, name, src, target, dst=None, when=None):
+        self.sent.append((name, src, target, dst, when))
+        perhaps(when, lambda: self._make(name, src(), target, dst and dst()).start())
+
+    def arrived(self, name, ref, source, when=None):
+        perhaps(when, lambda: self._make(name, ref(), source).wait_recv())
+
+    def drain(self):
+        for name, src, target, dst, when in self.sent:
+            perhaps(when, lambda: self._make(name, src(), target, dst and dst()).wait_send())
+        self.sent = []
+
+
+def perhaps(when, call):
+    if when is None:
+        call()
+    else:
+        pl.when(when)(call)
+
+
+def greet(targets):
+    barrier = pltpu.get_barrier_semaphore()
+    for target in targets:
+        pl.semaphore_signal(barrier, inc=1, device_id=target, device_id_type=MESH)
+    pl.semaphore_wait(barrier, len(targets))
+
+
+def whole_kernel(
+    group, source_ref, target_ref, key_ref, value_ref, query_ref, out_ref, source_gain_ref,
+    target_gain_ref, final_gain_ref, temp_ref,
+    result_ref,
+    blocks, normed, weights, small, early, late, query, total, tops, sums, partial, pieces,
+    from_core, from_first, from_second, relay, state,
+    send_sems, recv_sems, weight_sems,
+):
+    me = Place()
+    z, y, x, core = me.z, me.y, me.x, me.core
+    width = weights.shape[0]
+    side, wide = HEAD_DIM, group * HEAD_DIM
+    steps, positions = blocks.shape[0], math.prod(blocks.shape[1:5])
+    share, piece = normed.shape[5], blocks.shape[4]
+    count = 16 * share
+    span = pl.ds(pl.multiple_of(y * wide, wide), wide)
+
+    def plane(c, zz):
+        return blocks.at[c * 4 + zz]
+
+    def column(c, yy, xx):
+        return blocks.at[8 + c * 4 + yy * 2 + xx]
+
+    fetches = []
+    for layer in range(2):
+        for part, ref in enumerate((key_ref, value_ref)):
+            n = 2 * layer + part
+            fetches.append(
+                pltpu.make_async_copy(
+                    ref.at[layer, :, pl.ds(pl.multiple_of(y * side, side), side)],
+                    weights.at[:, pl.ds(n * side, side)],
+                    weight_sems.at[n],
+                )
+            )
+
+    def query_fetch(layer, dst, sem):
+        return [pltpu.make_async_copy(query_ref.at[layer, :, span], dst, weight_sems.at[sem])]
+
+    def out_fetch(layer, dst, sem):
+        half = width // 2
+        return [
+            pltpu.make_async_copy(
+                out_ref.at[layer, span, pl.ds(k * half, half)],
+                dst.at[pl.ds(k * half, half)],
+                weight_sems.at[sem + k],
+            )
+            for k in range(2)
+        ]
+
+    late_query, late_out = weights.at[:, pl.ds(0, wide)], weights.at[:, pl.ds(wide, wide)]
+    query_0, out_0 = query_fetch(0, small, 4), out_fetch(0, small, 5)
+    query_1, out_1 = query_fetch(1, late_query, 7), out_fetch(1, late_out, 8)
+
+    def begin(copies):
+        for copy in copies:
+            copy.start()
+
+    def finish(copies):
+        for copy in copies:
+            copy.wait()
+
+    begin(fetches)
+    begin(query_0)
+    for c in range(2):
+        blocks[c * 4 + z, y, x, core] = unit_rows(source_ref[c]).astype(jnp.bfloat16)
+        blocks[8 + c * 4 + y * 2 + x, z // 2, z % 2, core] = unit_rows(source_ref[2 + c]).astype(
+            jnp.bfloat16
+        )
+        rows = target_ref[c].astype(jnp.float32)
+        state[c] = rows
+        normed[0, c, y, x, core] = (unit_rows(rows) * target_gain_ref[0:1]).astype(jnp.bfloat16)
+    greet([me.at(x=me.ox), me.at(y=me.oy), me.at(z=me.up), me.at(z=me.down), me.at(core=me.other)])
+
+    net = Copies(send_sems, recv_sems)
+    sibling, xmate, ymate = me.at(core=me.other), me.at(x=me.ox), me.at(y=me.oy)
+    above, below = me.at(z=me.up), me.at(z=me.down)
+    first, second = [xmate, ymate], [ymate, xmate]
+
+    def share_with(name, part, when=None):
+        net.start(name + "d", lambda: part(core), sibling, when=when)
+
+    def shared(name, part, when=None):
+        net.arrived(name + "d", lambda: part(me.other), sibling, when=when)
+
+    def pair(c, zz):
+        return lambda k: plane(c, zz).at[y, :, k] if c == 0 else plane(c, zz).at[:, x, k]
+
+    def mates(c, zz):
+        return lambda k: plane(c, zz).at[me.oy, :, k] if c == 0 else plane(c, zz).at[:, me.ox, k]
+
+    def spot(c, zz):
+        return lambda k: column(c, y, x).at[zz // 2, zz % 2, k]
+
+    def whole(c, yy, xx):
+        return lambda k: column(c, yy, xx).at[:, :, k]
+
+    a_own = [lambda k, c=c: plane(c, z).at[y, x, k] for c in range(2)]
+    a_one = [lambda k: plane(0, z).at[y, me.ox, k], lambda k: plane(1, z).at[me.oy, x, k]]
+    b_one = [whole(0, me.oy, x), whole(1, y, me.ox)]
+    b_two = [whole(0, y, me.ox), whole(1, me.oy, x)]
+    b_last = [whole(c, me.oy, me.ox) for c in range(2)]
+    t_own = [lambda k, c=c: normed.at[0, c, y, x, k] for c in range(2)]
+    t_one = [lambda k: normed.at[0, 0, y, me.ox, k], lambda k: normed.at[0, 1, me.oy, x, k]]
+    t_two = [lambda k: normed.at[0, 0, me.oy, :, k], lambda k: normed.at[0, 1, :, me.ox, k]]
+    t_have = [lambda k: normed.at[0, 0, y, :, k], lambda k: normed.at[0, 1, :, x, k]]
+    top = 3
+    hops = range(top + 1)
+    ways = {
+        "u": (below, above, [z - d for d in hops], [z >= d for d in hops]),
+        "w": (above, below, [z + d for d in hops], [z + d <= top for d in hops]),
+    }
+    more = {"u": z < top, "w": z > 0}
+    goes = {way: [jnp.logical_and(c, more[way]) for c in ways[way][3]] for way in ways}
+
+    def go(c, part, name):
+        for way, (_, ahead, _, _) in ways.items():
+            net.start(f"{name}{c}{way}1", lambda: part(core), ahead, when=more[way])
+
+    def pass_on(c, d, name, region):
+        for way, (behind, ahead, began, comes) in ways.items():
+            part = region(c, began[d])
+            net.arrived(f"{name}{c}{way}{d}", lambda: part(core), behind, when=comes[d])
+            if d < top:
+                net.start(
+                    f"{name}{c}{way}{d + 1}",
+                    lambda part=part: part(core),
+                    ahead,
+                    when=goes[way][d],
+                )
+            if name == "a":
+                net.start(
+                    f"a{c}{way}{d}m", lambda part=part: part(core), second[c], when=comes[d]
+                )
+            share_with(f"{name}{c}{way}{d}", part, when=comes[d])
+
+    for c in range(2):
+        net.start(f"a{c}1", lambda c=c: a_own[c](core), first[c])
+        go(c, spot(c, z), "b")
+    for c in range(2):
+        net.start(f"t{c}1", lambda c=c: t_own[c](core), first[c])
+        share_with(f"b{c}0", spot(c, z))
+        share_with(f"t{c}0", t_own[c])
+
+    def scale(n):
+        fetches[n].wait()
+        columns = pl.ds(n * side, side)
+
+        def body(i, carry):
+            block = pl.ds(i * 256, 256)
+            weights[block, columns] = (
+                weights[block, columns].astype(jnp.float32) * source_gain_ref[n // 2, block, :]
+            ).astype(jnp.bfloat16)
+            return carry
+
+        lax.fori_loop(0, width // 256, body, 0)
+
+    def own_planes():
+        for c in range(2):
+            net.arrived(f"a{c}m", lambda: mates(c, z)(core), second[c])
+            share_with(f"a{c}m", mates(c, z))
+        for c in range(2):
+            shared(f"a{c}0", pair(c, z))
+            shared(f"a{c}m", mates(c, z))
+
+    def planes_come(d):
+        for c in range(2):
+            pass_on(c, d, "a", pair)
+
+    def planes_done(d):
+        for c in range(2):
+            for way, (_, _, began, comes) in ways.items():
+                part = mates(c, began[d])
+                net.arrived(f"a{c}{way}{d}m", lambda: part(core), second[c], when=comes[d])
+                share_with(f"a{c}{way}{d}m", part, when=comes[d])
+        for c in range(2):
+            for way, (_, _, began, comes) in ways.items():
+                shared(f"a{c}{way}{d}", pair(c, began[d]), when=comes[d])
+                shared(f"a{c}{way}{d}m", mates(c, began[d]), when=comes[d])
+
+    def rows_done():
+        for c in range(2):
+            net.arrived(f"t{c}2", lambda: t_two[c](core), second[c])
+            share_with(f"t{c}2", t_two[c])
+
+    def columns_come(d):
+        for c in range(2):
+            pass_on(c, d, "b", spot)
+
+    def columns_go(name, targets):
+        for c in range(2):
+            part = whole(c, y, x)
+            net.start(f"b{c}{name}", lambda part=part: part(core), targets[c])
+
+    def columns_done():
+        for c in range(2):
+            shared(f"b{c}0", spot(c, z))
+            for d in range(1, top + 1):
+                for way, (_, _, began, comes) in ways.items():
+                    shared(f"b{c}{way}{d}", spot(c, began[d]), when=comes[d])
+
+    def columns_one():
+        for c in range(2):
+            net.arrived(f"b{c}y", lambda: b_one[c](core), second[c])
+            share_with(f"b{c}4", b_one[c])
+        for c in range(2):
+            shared(f"b{c}4", b_one[c])
+
+    def columns_relay():
+        for c in range(2):
+            net.start(f"b{c}z", lambda c=c: b_one[c](core), first[c])
+
+    def columns_two():
+        for c in range(2):
+            net.arrived(f"b{c}x", lambda: b_two[c](core), first[c])
+            share_with(f"b{c}5", b_two[c])
+        for c in range(2):
+            shared(f"b{c}5", b_two[c])
+
+    def columns_last():
+        for c in range(2):
+            net.arrived(f"b{c}z", lambda: b_last[c](core), first[c])
+            share_with(f"b{c}6", b_last[c])
+        for c in range(2):
+            shared(f"b{c}6", b_last[c])
+
+    scale(0)
+    scale(1)
+    scale(2)
+    for c in range(2):
+        net.arrived(f"a{c}1", lambda: a_one[c](core), first[c])
+        part = pair(c, z)
+        net.start(f"a{c}m", lambda part=part: part(core), second[c])
+        share_with(f"a{c}0", part)
+    columns_come(1)
+    for c in range(2):
+        net.arrived(f"t{c}1", lambda: t_one[c](core), first[c])
+        net.start(f"t{c}2", lambda c=c: t_have[c](core), second[c])
+        share_with(f"t{c}1", t_one[c])
+    columns_come(2)
+    for c in range(2):
+        go(c, pair(c, z), "a")
+    scale(3)
+
+    def project_rows(layer, ref):
+        rows = normed[layer].reshape(count, width)
+        for head in range(group):
+            factor = temp_ref[layer, y * group + head] * (HEAD_DIM ** (-0.5) * LOG2E)
+            query[head] = (
+                jnp.dot(
+                    rows,
+                    ref[:, head * side : (head + 1) * side],
+                    preferred_element_type=jnp.float32,
+                )
+                * factor
+            ).astype(jnp.bfloat16)
+        total[...] = jnp.zeros_like(total)
+        sums[...] = jnp.zeros_like(sums)
+        tops[...] = jnp.full_like(tops, FLOOR)
+
+    def attend(kv):
+        keys = kv[:, :, :side].reshape(-1, side)
+        values = kv[:, :, side:].reshape(-1, side)
+        units = [(head, pl.ds(r, UNIT)) for head in range(group) for r in range(0, count, UNIT)]
+
+        def score(head, block):
+            return lax.dot_general(
+                query[head, block],
+                keys,
+                (((1,), (1,)), ((), ())),
+                preferred_element_type=jnp.float32,
+            )
+
+        ahead = score(*units[0])
+        for k, (head, block) in enumerate(units):
+            scores = ahead
+            if k + 1 < len(units):
+                ahead = score(*units[k + 1])
+            old_top = tops[head, block, :1]
+            new_top = jnp.maximum(old_top, jnp.max(scores, axis=-1, keepdims=True))
+            shrink = jnp.exp2(old_top - new_top)
+            expo = jnp.exp2(scores - new_top)
+            tops[head, block] = jnp.broadcast_to(new_top, (UNIT, tops.shape[2]))
+            new_sum = sums[head, block, :1] * shrink + jnp.sum(expo, axis=-1, keepdims=True)
+            sums[head, block] = jnp.broadcast_to(new_sum, (UNIT, sums.shape[2]))
+            total[head, block] = total[head, block] * shrink + jnp.dot(
+                expo.astype(jnp.bfloat16), values, preferred_element_type=jnp.float32
+            )
+
+    def first_query():
+        rows_done()
+        for c in range(2):
+            for k, part in enumerate((t_own, t_one, t_two)):
+                shared(f"t{c}{k}", part[c])
+        finish(query_0)
+        project_rows(0, small)
+        begin(out_0)
+
+    handlers = {
+        0: [own_planes],
+        1: [lambda: columns_come(3), lambda: columns_go("y", second), first_query],
+        2: [columns_done],
+        3: [lambda: planes_come(1)],
+        4: [lambda: columns_go("x", first), columns_one],
+        6: [lambda: planes_come(2), lambda: planes_done(1)],
+        8: [columns_two],
+        9: [lambda: planes_come(3), columns_relay],
+        10: [lambda: planes_done(2)],
+        12: [lambda: planes_done(3)],
+        14: [columns_last],
+    }
+    low = z < 2
+    near = jnp.where(z == 0, 1, jnp.where(z == 1, 0, jnp.where(z == 2, 3, 2)))
+    next_one = jnp.where(low, 2, 1)
+    far = jnp.where(low, 3, 0)
+    order = [
+        z, 4 + z, 8 + y * 2 + x, 12 + y * 2 + x,
+        8 + me.oy * 2 + x, 12 + y * 2 + me.ox, near, 4 + near,
+        8 + y * 2 + me.ox, 12 + me.oy * 2 + x, next_one, 4 + next_one,
+        far, 4 + far, 8 + me.oy * 2 + me.ox, 12 + me.oy * 2 + me.ox,
+    ]
+
+    def step(s, carry):
+        for k, calls in handlers.items():
+
+            @pl.when(s == k)
+            def _():
+                for call in calls:
+                    call()
+
+        which = order[0]
+        for k in range(1, steps):
+            which = jnp.where(s == k, order[k], which)
+        block = blocks[which].reshape(positions, width)
+        for n in range(4):
+            made = jnp.dot(
+                block, weights[:, n * side : (n + 1) * side], preferred_element_type=jnp.float32
+            ).astype(jnp.bfloat16)
+            if n < 2:
+                early[s % 2, :, n * side : (n + 1) * side] = made
+            else:
+                late[s, :, (n - 2) * side : (n - 1) * side] = made
+
+        @pl.when(s % 2 == 1)
+        def _():
+            attend(early)
+
+        return carry
+
+    lax.fori_loop(0, steps, step, 0)
+    begin(query_1)
+    begin(out_1)
+
+    def out_rows(layer, ref, c):
+        block = slice(c * (count // 2), (c + 1) * (count // 2))
+        attended = jnp.concatenate(
+            [
+                (total[head, block] / sums[head, block, :1]).astype(jnp.bfloat16)
+                for head in range(group)
+            ],
+            axis=1,
+        )
+        half = width // 2
+        for k in range(2):
+            for n in range(0, half, side):
+                term = jnp.dot(
+                    attended,
+                    ref[k * half : (k + 1) * half, n : n + side],
+                    preferred_element_type=jnp.float32,
+                ).astype(jnp.bfloat16)
+                partial[c, :, :, :, :, k * half + n : k * half + n + side] = term.reshape(
+                    2, 2, 2, share, side
+                )
+
+    sides = [[me.oy, y], [me.ox, x]]
+    spots = [(x, me.ox), (y, me.oy)]
+
+    def piece_of(c, k, who):
+        return partial.at[c, sides[c][k], :, who] if c == 0 else partial.at[c, :, sides[c][k], who]
+
+    def fold_start(layer, c):
+        for k in range(2):
+            net.start(
+                f"c{c}{k}{layer}",
+                lambda c=c, k=k: piece_of(c, k, me.other),
+                sibling,
+                lambda c=c, k=k: from_core.at[layer, c, k],
+            )
+
+    def fold_pairs(layer):
+        for k in range(2):
+            for c in range(2):
+                net.arrived(f"c{c}{k}{layer}", lambda: from_core.at[layer, c, k], sibling)
+                pieces[c, k] = (
+                    piece_of(c, k, core)[...].astype(jnp.float32)
+                    + from_core[layer, c, k].astype(jnp.float32)
+                ).astype(jnp.bfloat16)
+                if k == 0:
+                    net.start(
+                        f"p{c}{layer}",
+                        lambda c=c: pieces.at[c, 0],
+                        second[c],
+                        lambda c=c: from_first.at[layer, c],
+                    )
+        for c in range(2):
+            far = spots[c][1]
+            net.arrived(f"p{c}{layer}", lambda: from_first.at[layer, c], second[c])
+            relay[c] = (
+                pieces[c, 1, far].astype(jnp.float32) + from_first[layer, c, far].astype(jnp.float32)
+            ).astype(jnp.bfloat16)
+            net.start(
+                f"q{c}{layer}",
+                lambda c=c: relay.at[c],
+                first[c],
+                lambda c=c: from_second.at[layer, c],
+            )
+
+    def folded(layer, c):
+        near = spots[c][0]
+        partly = pieces[c, 1, near].astype(jnp.float32) + from_first[layer, c, near].astype(
+            jnp.float32
+        )
+        net.arrived(f"q{c}{layer}", lambda: from_second.at[layer, c], first[c])
+        return state[c] + (partly + from_second[layer, c].astype(jnp.float32))
+
+    finish(out_0)
+    for c in range(2):
+        out_rows(0, small, c)
+        fold_start(0, c)
+    fold_pairs(0)
+    own = [lambda k, c=c: normed.at[1, c, y, x, k] for c in range(2)]
+    one = [lambda k: normed.at[1, 0, y, me.ox, k], lambda k: normed.at[1, 1, me.oy, x, k]]
+    two = [lambda k: normed.at[1, 0, me.oy, :, k], lambda k: normed.at[1, 1, :, me.ox, k]]
+    have = [lambda k: normed.at[1, 0, y, :, k], lambda k: normed.at[1, 1, :, x, k]]
+    for c in range(2):
+        rows = folded(0, c)
+        state[c] = rows
+        normed[1, c, y, x, core] = (unit_rows(rows) * target_gain_ref[1:2]).astype(jnp.bfloat16)
+        net.start(f"n{c}1", lambda c=c: own[c](core), first[c])
+        share_with(f"n{c}0", own[c])
+    for c in range(2):
+        net.arrived(f"n{c}1", lambda: one[c](core), first[c])
+        net.start(f"n{c}2", lambda c=c: have[c](core), second[c])
+        share_with(f"n{c}1", one[c])
+    for c in range(2):
+        net.arrived(f"n{c}2", lambda: two[c](core), second[c])
+        share_with(f"n{c}2", two[c])
+    for c in range(2):
+        for k, part in enumerate((own, one, two)):
+            shared(f"n{c}{k}", part[c])
+    net.drain()
+    finish(query_1)
+    project_rows(1, late_query)
+
+    def second_step(j, carry):
+        attend(late.at[pl.ds(4 * j, 4)])
+        return carry
+
+    lax.fori_loop(0, steps // 4, second_step, 0)
+    finish(out_1)
+    for c in range(2):
+        out_rows(1, late_out, c)
+        fold_start(1, c)
+    fold_pairs(1)
+    for c in range(2):
+        result_ref[c] = unit_rows(folded(1, c)) * final_gain_ref[...]
+    net.drain()
+
+
+def on_planes(
+    target, source, target_gain, source_gain, query_w, key_w, value_w, out_w, head_temp, final_gain
+):
+    width = target.shape[1]
+    group = query_w.shape[2] // key_w.shape[2]
+    piece, share = source.shape[0] // 4, target.shape[0] // 2
+    count, positions, copies = 16 * share, 8 * piece, 140
+    part = (2, share, width)
+    return pl.pallas_call(
+        functools.partial(whole_kernel, group),
+        out_shape=jax.ShapeDtypeStruct(part, jnp.float32),
+        in_specs=[VMEM, VMEM, HBM, HBM, HBM, HBM, VMEM, VMEM, VMEM, SMEM],
+        out_specs=VMEM,
+        scratch_shapes=[
+            pltpu.VMEM((16, 2, 2, 2, piece, width), jnp.bfloat16),
+            pltpu.VMEM((2, 2, 2, 2, 2, share, width), jnp.bfloat16),
+            pltpu.VMEM((width, 4 * HEAD_DIM), jnp.bfloat16),
+            pltpu.VMEM((width, group * HEAD_DIM), jnp.bfloat16),
+            pltpu.VMEM((2, positions, 2 * HEAD_DIM), jnp.bfloat16),
+            pltpu.VMEM((16, positions, 2 * HEAD_DIM), jnp.bfloat16),
+            pltpu.VMEM((group, count, HEAD_DIM), jnp.bfloat16),
+            pltpu.VMEM((group, count, HEAD_DIM), jnp.float32),
+            pltpu.VMEM((group, count, 128), jnp.float32),
+            pltpu.VMEM((group, count, 128), jnp.float32),
+            pltpu.VMEM((2, 2, 2, 2, share, width), jnp.bfloat16),
+            pltpu.VMEM((2, 2, 2, share, width), jnp.bfloat16),
+            pltpu.VMEM((2, 2, 2, 2, share, width), jnp.bfloat16),
+            pltpu.VMEM((2, 2, 2, share, width), jnp.bfloat16),
+            pltpu.VMEM((2, 2, share, width), jnp.bfloat16),
+            pltpu.VMEM((2, share, width), jnp.bfloat16),
+            pltpu.VMEM(part, jnp.float32),
+            pltpu.SemaphoreType.DMA((copies,)),
+            pltpu.SemaphoreType.DMA((copies,)),
+            pltpu.SemaphoreType.DMA((10,)),
+        ],
+        compiler_params=pltpu.CompilerParams(
+            collective_id=0, has_side_effects=True, vmem_limit_bytes=63 * MIB
+        ),
+    )(
+        source.reshape(4, piece, width),
+        target.reshape(2, share, width),
+        key_w,
+        value_w,
+        query_w,
+        out_w,
+        source_gain.astype(jnp.float32)[:, :, None],
+        target_gain.astype(jnp.float32),
+        final_gain.astype(jnp.float32).reshape(1, width),
+        head_temp,
+    ).reshape(-1, width)
 
 
 def shifted(block, shift):
@@ -40,7 +626,7 @@
     return mixed
 
 
-def attend_kernel(rows, query_ref, source_ref, mix_ref, total_ref, top_ref, sum_ref):
+def flash_kernel(rows, query_ref, source_ref, mix_ref, total_ref, top_ref, sum_ref):
     step = pl.program_id(0)
     count = query_ref.shape[0]
 
@@ -82,7 +668,7 @@
     chunk = math.gcd(chunk, positions)
     rows = math.gcd(rows, count)
     return pl.pallas_call(
-        functools.partial(attend_kernel, rows),
+        functools.partial(flash_kernel, rows),
         grid=(positions // chunk,),
         out_shape=jax.ShapeDtypeStruct((count, width), jnp.bfloat16),
         in_specs=[
@@ -166,6 +752,10 @@
     return unit_rows(hidden_state) * final_gain.astype(jnp.float32)
 
 
+def fits(mesh):
+    return dict(mesh.shape) == {"sp": 8, "tp": 4}
+
+
 def solution(mesh):
     in_specs = (
         P(("sp", "tp"), None),
@@ -181,5 +771,5 @@
     )
     out_specs = P(("sp", "tp"), None)
     return jax.shard_map(
-        per_device, mesh=mesh, in_specs=in_specs, out_specs=out_specs, check_vma=False
+        on_planes if fits(mesh) else per_device, mesh=mesh, in_specs=in_specs, out_specs=out_specs, check_vma=False
     )

time: 322 us -> 165 us (0.51)
  waiting for transfers between devices: 121 us -> 0 us
  Pallas kernels: 112 us -> 157 us
  matrix products: 31.5 us -> 0 us
  between operations: 13.7 us -> 0.01 us
  local copies, waits for them, and re-layouts: 16.9 us -> 3.87 us
  starting transfers between devices: 11.8 us -> 0 us
  other arithmetic: 15 us -> 3.29 us
    all_gather x1 -> x0, waiting for transfers between devices: 85.9 us -> none  [per_device(): lax.all_gather(unit_rows(source).astype(jnp.bfloat16), ('sp', 'tp'), axis...]
    pallas_call x2 -> x1, Pallas kernels: 112 us -> 157 us  [on_planes(): pl.pallas_call(functools.partial(whole_kernel, group), out_shape=jax.Shap...]
    ppermute x12 -> x0, waiting for transfers between devices: 35 us -> none  [shifted(): lax.ppermute(block, 'tp', [(i, (i + shift) % size) for i in range(size)])]
    dot_general x20 -> x0, matrix products: 31.5 us -> none  [the longest x2 12.1 us: per_device(): jnp.dot(jnp.concatenate(attended, axis=1), out_w[layer], preferred_elemen...]
    ppermute x12 -> x0, starting transfers between devices: 11.8 us -> none  [shifted(): lax.ppermute(block, 'tp', [(i, (i + shift) % size) for i in range(size)])]
    squeeze x2 -> x0, local copies, waits for them, and re-layouts: 10.4 us -> none  [the longest x1 5.86 us: per_device(): key_w[layer][:, columns]]
    mul x4 -> x0, other arithmetic: 5.91 us -> none  [the longest x1 4.89 us: per_device(): gain * scales[head]]
    concatenate x2 -> x0, other arithmetic: 4.84 us -> none  [per_device(): mix = attend(jnp.concatenate(lifted, axis=0), positions)]
  transfers between devices with their start and end apart: 13 -> 0, of which waited for: 8 -> 0; matrix products, arithmetic and copies ran while one was open for 7% -> 0% of each run, Pallas kernels for 0% -> 0%
where the time goes in v2:
time: 165 us; the launch traced here: 164 us
  Pallas kernels  157 us (95%)
  local copies, waits for them, and re-layouts  3.87 us (2%)
  other arithmetic  3.29 us (2%)
    pallas_call x1, Pallas kernels, on_planes(): pl.pallas_call(functools.partial(whole_kernel, group), out_shape=jax.Shap...  157 us

profile of v2, /device:TPU:0, one launch (start us, length us, event | category | flops | bytes accessed | tf_op | source)
XLA Modules:
  0.0 164.3 jit_solution(14743564089815108803)
XLA Ops:
  0.0 1.3 reshape.20
  1.3 1.3 convert_element_type.2.target_gain_ref
  2.6 0.7 bitcast_convert_fusion
  3.3 2.0 %copy.11.source_gain_ref = f32[2,2048,1]{2,1,0:T(8,128)} copy(f32[2,2048,1]{1,0,2:T(2,128)S(1)} %bitcast_convert_fusion) | data formatting | bytes 32768 | tf_op jit(solution)/shard_map/broadcast_in_dim | solution.py:603
  5.3 157.1 %shard_map.100 = f32[2,32,2048]{2,1,0:T(8,128)} custom-call(bf16[4,32,2048]{2,1,0:T(8,128)(2,1)} %bitcast.8, bf16[2,32,2048]{2,1,0:T(8,128)(2,1)} %bitcast.9, bf16[2,2048,1024]{2,1,0:T(8,128)(2,1)} %key_ref.1, bf16[2,2048,1024]{2,1,0:T(8,128)(2,1)} %value_ref.1, bf16[2,2048,2048]{2,1,0:T(8,128)(2,1)} %query_ref.1, bf16[2,2048,2048]{2,1,0:T(8,128)(2,1)} %out_ref.1, ...), custom_call_target="tpu_custom_call" | custom-call | tf_op jit(solution)/shard_map/pallas_call | solution.py:566
  162.4 1.9 %copy.13 = f32[64,2048]{1,0:T(8,128)} copy(f32[64,2048]{1,0:T(8,128)} %bitcast.7) | data formatting | bytes 1048576

commit v3 on v2

--- a/solution.py
+++ b/solution.py
@@ -15,6 +15,7 @@
 ROWS = 512
 UNIT = 256
 LOG2E = math.log2(math.e)
+LATER = 12
 MESH = pl.DeviceIdType.MESH
 MIB = 1024 * 1024
 HBM = pl.BlockSpec(memory_space=pl.ANY)
@@ -148,16 +149,19 @@
         for copy in copies:
             copy.wait()
 
+    target_gain = target_gain_ref[...].astype(jnp.float32)
     begin(fetches)
     begin(query_0)
     for c in range(2):
-        blocks[c * 4 + z, y, x, core] = unit_rows(source_ref[c]).astype(jnp.bfloat16)
-        blocks[8 + c * 4 + y * 2 + x, z // 2, z % 2, core] = unit_rows(source_ref[2 + c]).astype(
+        of_plane = source_ref[c * piece : (c + 1) * piece]
+        of_column = source_ref[(2 + c) * piece : (3 + c) * piece]
+        blocks[c * 4 + z, y, x, core] = unit_rows(of_plane).astype(jnp.bfloat16)
+        blocks[8 + c * 4 + y * 2 + x, z // 2, z % 2, core] = unit_rows(of_column).astype(
             jnp.bfloat16
         )
-        rows = target_ref[c].astype(jnp.float32)
+        rows = target_ref[c * share : (c + 1) * share].astype(jnp.float32)
         state[c] = rows
-        normed[0, c, y, x, core] = (unit_rows(rows) * target_gain_ref[0:1]).astype(jnp.bfloat16)
+        normed[0, c, y, x, core] = (unit_rows(rows) * target_gain[0:1]).astype(jnp.bfloat16)
     greet([me.at(x=me.ox), me.at(y=me.oy), me.at(z=me.up), me.at(z=me.down), me.at(core=me.other)])
 
     net = Copies(send_sems, recv_sems)
@@ -235,13 +239,15 @@
         columns = pl.ds(n * side, side)
 
         def body(i, carry):
-            block = pl.ds(i * 256, 256)
+            block = pl.ds(pl.multiple_of(i * 128, 128), 128)
+            gain = source_gain_ref[:, block].astype(jnp.float32)[n // 2 : n // 2 + 1]
+            gain = jnp.transpose(jnp.broadcast_to(gain, (128, 128)))[:, :1]
             weights[block, columns] = (
-                weights[block, columns].astype(jnp.float32) * source_gain_ref[n // 2, block, :]
+                weights[block, columns].astype(jnp.float32) * gain
             ).astype(jnp.bfloat16)
             return carry
 
-        lax.fori_loop(0, width // 256, body, 0)
+        lax.fori_loop(0, width // 128, body, 0)
 
     def own_planes():
         for c in range(2):
@@ -408,6 +414,25 @@
         far, 4 + far, 8 + me.oy * 2 + me.ox, 12 + me.oy * 2 + me.ox,
     ]
 
+    kept = steps - LATER
+
+    def block_at(s):
+        which = order[0]
+        for k in range(1, steps):
+            which = jnp.where(s == k, order[k], which)
+        return blocks[which].reshape(positions, width)
+
+    def made(block, n):
+        return jnp.dot(
+            block, weights[:, n * side : (n + 1) * side], preferred_element_type=jnp.float32
+        ).astype(jnp.bfloat16)
+
+    def project_late(s, carry=0):
+        block = block_at(s)
+        for n in range(2):
+            late[s, :, n * side : (n + 1) * side] = made(block, 2 + n)
+        return carry
+
     def step(s, carry):
         for k, calls in handlers.items():
 
@@ -416,18 +441,13 @@
                 for call in calls:
                     call()
 
-        which = order[0]
-        for k in range(1, steps):
-            which = jnp.where(s == k, order[k], which)
-        block = blocks[which].reshape(positions, width)
-        for n in range(4):
-            made = jnp.dot(
-                block, weights[:, n * side : (n + 1) * side], preferred_element_type=jnp.float32
-            ).astype(jnp.bfloat16)
-            if n < 2:
-                early[s % 2, :, n * side : (n + 1) * side] = made
-            else:
-                late[s, :, (n - 2) * side : (n - 1) * side] = made
+        block = block_at(s)
+        for n in range(2):
+            early[s % 2, :, n * side : (n + 1) * side] = made(block, n)
+
+        @pl.when(s < kept)
+        def _():
+            project_late(s)
 
         @pl.when(s % 2 == 1)
         def _():
@@ -437,7 +457,11 @@
 
     lax.fori_loop(0, steps, step, 0)
     begin(query_1)
-    begin(out_1)
+    waits = iter(range(4))
+
+    def meanwhile():
+        k, each = next(waits), LATER // 4
+        lax.fori_loop(kept + k * each, kept + (k + 1) * each, project_late, 0)
 
     def out_rows(layer, ref, c):
         block = slice(c * (count // 2), (c + 1) * (count // 2))
@@ -475,7 +499,7 @@
                 lambda c=c, k=k: from_core.at[layer, c, k],
             )
 
-    def fold_pairs(layer):
+    def fold_pairs(layer, between=lambda: None):
         for k in range(2):
             for c in range(2):
                 net.arrived(f"c{c}{k}{layer}", lambda: from_core.at[layer, c, k], sibling)
@@ -490,6 +514,7 @@
                         second[c],
                         lambda c=c: from_first.at[layer, c],
                     )
+        between()
         for c in range(2):
             far = spots[c][1]
             net.arrived(f"p{c}{layer}", lambda: from_first.at[layer, c], second[c])
@@ -515,7 +540,8 @@
     for c in range(2):
         out_rows(0, small, c)
         fold_start(0, c)
-    fold_pairs(0)
+    fold_pairs(0, meanwhile)
+    meanwhile()
     own = [lambda k, c=c: normed.at[1, c, y, x, k] for c in range(2)]
     one = [lambda k: normed.at[1, 0, y, me.ox, k], lambda k: normed.at[1, 1, me.oy, x, k]]
     two = [lambda k: normed.at[1, 0, me.oy, :, k], lambda k: normed.at[1, 1, :, me.ox, k]]
@@ -523,13 +549,16 @@
     for c in range(2):
         rows = folded(0, c)
         state[c] = rows
-        normed[1, c, y, x, core] = (unit_rows(rows) * target_gain_ref[1:2]).astype(jnp.bfloat16)
+        normed[1, c, y, x, core] = (unit_rows(rows) * target_gain[1:2]).astype(jnp.bfloat16)
         net.start(f"n{c}1", lambda c=c: own[c](core), first[c])
         share_with(f"n{c}0", own[c])
+    meanwhile()
     for c in range(2):
         net.arrived(f"n{c}1", lambda: one[c](core), first[c])
         net.start(f"n{c}2", lambda c=c: have[c](core), second[c])
         share_with(f"n{c}1", one[c])
+    meanwhile()
+    begin(out_1)
     for c in range(2):
         net.arrived(f"n{c}2", lambda: two[c](core), second[c])
         share_with(f"n{c}2", two[c])
@@ -551,7 +580,8 @@
         fold_start(1, c)
     fold_pairs(1)
     for c in range(2):
-        result_ref[c] = unit_rows(folded(1, c)) * final_gain_ref[...]
+        rows = unit_rows(folded(1, c)) * final_gain_ref[...].astype(jnp.float32)
+        result_ref[c * share : (c + 1) * share] = rows
     net.drain()
 
 
@@ -565,7 +595,7 @@
     part = (2, share, width)
     return pl.pallas_call(
         functools.partial(whole_kernel, group),
-        out_shape=jax.ShapeDtypeStruct(part, jnp.float32),
+        out_shape=jax.ShapeDtypeStruct(target.shape, jnp.float32),
         in_specs=[VMEM, VMEM, HBM, HBM, HBM, HBM, VMEM, VMEM, VMEM, SMEM],
         out_specs=VMEM,
         scratch_shapes=[
@@ -594,17 +624,17 @@
             collective_id=0, has_side_effects=True, vmem_limit_bytes=63 * MIB
         ),
     )(
-        source.reshape(4, piece, width),
-        target.reshape(2, share, width),
+        source,
+        target,
         key_w,
         value_w,
         query_w,
         out_w,
-        source_gain.astype(jnp.float32)[:, :, None],
-        target_gain.astype(jnp.float32),
-        final_gain.astype(jnp.float32).reshape(1, width),
+        source_gain,
+        target_gain,
+        final_gain.reshape(1, width),
         head_temp,
-    ).reshape(-1, width)
+    )
 
 
 def shifted(block, shift):

time: 165 us -> 154 us (0.933)
  Pallas kernels: 157 us -> 151 us
  other arithmetic: 3.29 us -> 0 us
    pallas_call x1, Pallas kernels: 157 us -> 151 us  [on_planes(): pl.pallas_call(functools.partial(whole_kernel, group), out_shape=jax.Shap...]
    broadcast_in_dim x1 -> x0, local copies, waits for them, and re-layouts: 2 us -> none  [on_planes(): source_gain.astype(jnp.float32)[:, :, None]]
where the time goes in v3:
time: 154 us
  Pallas kernels  151 us (98%)
  local copies, waits for them, and re-layouts  3.16 us (2%)
    pallas_call x1, Pallas kernels, on_planes(): pl.pallas_call(functools.partial(whole_kernel, group), out_shape=jax.Shap...  151 us

profile of v3, /device:TPU:0, one launch (start us, length us, event | category | flops | bytes accessed | tf_op | source)
XLA Modules:
  0.0 153.9 jit_solution(14711223116775401814)
XLA Ops:
  0.0 1.3 reshape.3.final_gain_ref
  1.3 150.8 %shard_map.100 = f32[64,2048]{1,0:T(8,128)} custom-call(bf16[128,2048]{1,0:T(8,128)(2,1)} %source_ref.1, bf16[64,2048]{1,0:T(8,128)(2,1)} %target_ref.1, bf16[2,2048,1024]{2,1,0:T(8,128)(2,1)} %key_ref.1, bf16[2,2048,1024]{2,1,0:T(8,128)(2,1)} %value_ref.1, bf16[2,2048,2048]{2,1,0:T(8,128)(2,1)} %query_ref.1, bf16[2,2048,2048]{2,1,0:T(8,128)(2,1)} %out_ref.1, ...), custom_call_target="tpu_custom_call" | custom-call | tf_op jit(solution)/shard_map/pallas_call | solution.py:596
  152.1 1.9 %copy.12 = f32[64,2048]{1,0:T(8,128)} copy(f32[64,2048]{1,0:T(8,128)} %shard_map.100) | data formatting | bytes 1048576

commit v4 on v3

--- a/solution.py
+++ b/solution.py
@@ -85,7 +85,7 @@
     barrier = pltpu.get_barrier_semaphore()
     for target in targets:
         pl.semaphore_signal(barrier, inc=1, device_id=target, device_id_type=MESH)
-    pl.semaphore_wait(barrier, len(targets))
+    return lambda: pl.semaphore_wait(barrier, len(targets))
 
 
 def whole_kernel(
@@ -150,6 +150,7 @@
             copy.wait()
 
     target_gain = target_gain_ref[...].astype(jnp.float32)
+    all_here = greet([me.at(x=me.ox), me.at(y=me.oy), me.at(z=me.up), me.at(z=me.down), me.at(core=me.other)])
     begin(fetches)
     begin(query_0)
     for c in range(2):
@@ -162,7 +163,7 @@
         rows = target_ref[c * share : (c + 1) * share].astype(jnp.float32)
         state[c] = rows
         normed[0, c, y, x, core] = (unit_rows(rows) * target_gain[0:1]).astype(jnp.bfloat16)
-    greet([me.at(x=me.ox), me.at(y=me.oy), me.at(z=me.up), me.at(z=me.down), me.at(core=me.other)])
+    all_here()
 
     net = Copies(send_sems, recv_sems)
     sibling, xmate, ymate = me.at(core=me.other), me.at(x=me.ox), me.at(y=me.oy)

time: 154 us -> 154 us (level)
  no operation moved by 1% of the time
where the time goes in v4:
time: 154 us
  Pallas kernels  151 us (98%)
  local copies, waits for them, and re-layouts  3.16 us (2%)
    pallas_call x1, Pallas kernels, on_planes(): pl.pallas_call(functools.partial(whole_kernel, group), out_shape=jax.Shap...  151 us

profile of v4, /device:TPU:0, one launch (start us, length us, event | category | flops | bytes accessed | tf_op | source)
XLA Modules:
  0.0 154.1 jit_solution(8502766861787469302)
XLA Ops:
  0.0 1.3 reshape.3.final_gain_ref
  1.3 150.9 %shard_map.100 = f32[64,2048]{1,0:T(8,128)} custom-call(bf16[128,2048]{1,0:T(8,128)(2,1)} %source_ref.1, bf16[64,2048]{1,0:T(8,128)(2,1)} %target_ref.1, bf16[2,2048,1024]{2,1,0:T(8,128)(2,1)} %key_ref.1, bf16[2,2048,1024]{2,1,0:T(8,128)(2,1)} %value_ref.1, bf16[2,2048,2048]{2,1,0:T(8,128)(2,1)} %query_ref.1, bf16[2,2048,2048]{2,1,0:T(8,128)(2,1)} %out_ref.1, ...), custom_call_target="tpu_custom_call" | custom-call | tf_op jit(solution)/shard_map/pallas_call | solution.py:597
  152.2 1.9 %copy.12 = f32[64,2048]{1,0:T(8,128)} copy(f32[64,2048]{1,0:T(8,128)} %shard_map.100) | data formatting | bytes 1048576
